TPU v7x, 512 devices: a 4x2x32 block of a 4x8x32 slice. The times are simulated.
512 devices in a mesh: grp: 2 (over y), sp: 32 (over z), tp: 8 (over x, core).
Axes of the slice: x: 4, y: 2, z: 32, core: 2. Of those that a mesh axis runs over, the one named last changes fastest.
The devices are a block of a 4x8x32 slice.
Arguments:
- query_rows: bfloat16 [8192, 1024], P(('grp', 'sp'), 'tp'), parts along dimension 0, may hold values from -12 to 12
- key_rows: bfloat16 [8192, 1024], P(('grp', 'sp'), 'tp'), parts along dimension 0, may hold values from -9 to 9
- value_rows: bfloat16 [8192, 1024], P(('grp', 'sp'), 'tp'), parts along dimension 0, may hold values from -6 to 6
- key_logit: bfloat16 [8192, 8], P(('grp', 'sp'), 'tp'), parts along dimension 0, as said below
- residual: bfloat16 [8192, 2048], P(('grp', 'sp')), parts along dimension 0, may hold values from -6 to 6
- out_weight: bfloat16 [1024, 2048], P('tp'), may hold values from -0.1875 to 0.1875
- mix_gain: float32 [2048], replicated, may hold values from 0.1 to 1.9
- ffn_gain: float32 [2048], replicated, may hold values from 0.1 to 1.9
- out_gain: float32 [2048], replicated, may hold values from 0.1 to 1.9
- gate_weight: bfloat16 [2048, 5120], P('sp', 'tp'), may hold values from -0.125 to 0.125
- up_weight: bfloat16 [2048, 5120], P('sp', 'tp'), may hold values from -0.125 to 0.125
- down_weight: bfloat16 [2048, 5120], P('sp', 'tp'), may hold values from -0.078125 to 0.078125
Outputs:
- layer_out: bfloat16 [8192, 2048], P(('grp', 'sp')), parts along dimension 0
There are 2 independent parts, one for each index of `grp`. A program takes and returns all parts, laid end to end along the dimension named above; an argument that names none is the same for every part. Nothing has to cross between parts.
Inputs may be any that keep to these rules, and one draw needn't show every extreme that they name: `key_logit`: log-odds offsets of the keys, all negative.
All inputs are finite; a program needn't handle non-finite values.
Results may differ from a plain program's by a relative error of at most 0.018.
Values may be sent and summed in bfloat16 or wider, within the bound.
A program may use at most 64 MiB of HBM per device.

v0:
```python
import jax
import jax.numpy as jnp
from jax import lax
from jax.sharding import PartitionSpec as P

epsilon = 1e-06


def sent_together(arrays, axis, dim, along):
    widths = [a.shape[along] for a in arrays]
    both = jnp.concatenate(arrays, axis=along)
    result = lax.all_gather(both, axis, axis=dim, tiled=True)
    return tuple(jnp.split(result, [sum(widths[:k]) for k in range(1, len(widths))], axis=along))


def sent_to_all(x, axis):
    count = lax.axis_size(axis)
    return lax.all_to_all(jnp.broadcast_to(x[None], (count, *x.shape)), axis, 0, 0, tiled=True)


def over_copies(x, axis):
    everything = sent_to_all(x, axis)
    return jnp.sum(everything.astype(jnp.float32), axis=0)


def total_of_pieces(x, axis):
    return lax.all_gather(x, axis).astype(jnp.float32).sum(0)


def normalize(payload_table):
    return payload_table * lax.rsqrt(
        jnp.mean(payload_table * payload_table, axis=-1, keepdims=True) + epsilon
    )


def shards(
    query_rows,
    key_rows,
    value_rows,
    key_logit,
    residual,
    out_weight,
    mix_gain,
    ffn_gain,
    out_gain,
    gate_weight,
    up_weight,
    down_weight,
):
    tok_rows = query_rows.shape[0]
    head_count = key_logit.shape[1]
    head_width = query_rows.shape[1] // head_count
    block_count = lax.axis_size("sp")
    own_block = lax.axis_index("sp")
    whole_gate, whole_up, whole_down = sent_together(
        (gate_weight, up_weight, down_weight), "sp", 0, 1
    )
    queries = query_rows.reshape(tok_rows, head_count, head_width).transpose(1, 0, 2)
    score_scale = head_width ** (-0.5)
    query_pos = own_block * tok_rows + jnp.arange(tok_rows, dtype=jnp.int32)[:, None]

    def group_terms(key_part, value_part, logit_part, first_block):
        span_rows = key_part.shape[0]
        shard_count = span_rows // tok_rows

        def compute(unused):
            scores = (
                jnp.einsum(
                    "hqd,khd->hqk",
                    queries,
                    key_part.reshape(span_rows, head_count, head_width),
                    preferred_element_type=jnp.float32,
                )
                * score_scale
            )
            scores = scores + jnp.transpose(logit_part.astype(jnp.float32))[:, None, :]
            key_pos = first_block * tok_rows + jnp.arange(span_rows, dtype=jnp.int32)[None, :]
            causal = (key_pos < query_pos).reshape(tok_rows, shard_count, tok_rows)
            scores = scores.reshape(head_count, tok_rows, shard_count, tok_rows)
            keep_log = jnp.where(causal, jax.nn.log_sigmoid(-scores), 0.0)
            within = lax.cumsum(keep_log, axis=3, reverse=True) - keep_log
            sticks = jnp.where(causal, jnp.exp(jax.nn.log_sigmoid(scores) + within), 0.0).astype(
                jnp.bfloat16
            )
            partials = jnp.einsum(
                "hqgk,gkhd->ghqd",
                sticks,
                value_part.reshape(shard_count, tok_rows, head_count, head_width),
                preferred_element_type=jnp.float32,
            )
            return (jnp.sum(keep_log, axis=3), partials)

        def skipped(unused):
            return (
                jnp.zeros((head_count, tok_rows, shard_count), jnp.float32),
                jnp.zeros((shard_count, head_count, tok_rows, head_width), jnp.float32),
            )

        return lax.cond(first_block <= own_block, compute, skipped, 0)

    initial = (
        jnp.zeros((head_count, tok_rows, block_count), jnp.float32),
        jnp.zeros((block_count, head_count, tok_rows, head_width), jnp.float32),
    )
    tables = initial
    key_part, value_part, logit_part = sent_together((key_rows, value_rows, key_logit), "sp", 0, 1)
    shard_count = key_part.shape[0] // tok_rows
    group_size = 2
    span_rows = group_size * tok_rows

    def one_group(carried, group_index):
        offset = group_index * span_rows
        first_block = group_index * group_size
        totals, partials = group_terms(
            lax.dynamic_slice_in_dim(key_part, offset, span_rows, 0),
            lax.dynamic_slice_in_dim(value_part, offset, span_rows, 0),
            lax.dynamic_slice_in_dim(logit_part, offset, span_rows, 0),
            first_block,
        )
        carried = (
            lax.dynamic_update_slice(carried[0], totals, (0, 0, first_block)),
            lax.dynamic_update_slice(carried[1], partials, (first_block, 0, 0, 0)),
        )
        return (carried, None)

    tables, unused = lax.scan(
        one_group, tables, jnp.arange(shard_count // group_size, dtype=jnp.int32)
    )
    totals, partials = tables
    suffix = lax.cumsum(totals, axis=2, reverse=True) - totals
    attended = jnp.einsum(
        "hqb,bhqd->qhd", jnp.exp(suffix), partials, precision=lax.Precision.HIGHEST
    )
    attended = attended.reshape(tok_rows, head_count * head_width).astype(jnp.bfloat16)
    head_part = jnp.dot(attended, out_weight, preferred_element_type=jnp.float32)
    mixed_rows = (
        over_copies(head_part.astype(jnp.bfloat16), "tp").astype(jnp.float32).astype(jnp.bfloat16)
    )
    middle = (
        residual.astype(jnp.float32) + mix_gain * normalize(mixed_rows.astype(jnp.float32))
    ).astype(jnp.bfloat16)
    normed = (ffn_gain * normalize(middle.astype(jnp.float32))).astype(jnp.bfloat16)
    gate_act = jnp.dot(normed, whole_gate, preferred_element_type=jnp.float32)
    up_act = jnp.dot(normed, whole_up, preferred_element_type=jnp.float32)
    hidden = (jax.nn.silu(gate_act) * up_act).astype(jnp.bfloat16)
    unit_part = lax.dot_general(
        hidden, whole_down, (((1,), (1,)), ((), ())), preferred_element_type=jnp.float32
    )
    ffn_out = (
        total_of_pieces(unit_part.astype(jnp.bfloat16), "tp")
        .astype(jnp.float32)
        .astype(jnp.bfloat16)
    )
    return (middle.astype(jnp.float32) + out_gain * normalize(ffn_out.astype(jnp.float32))).astype(
        jnp.bfloat16
    )


def solution(mesh):
    placed = (
        P(("grp", "sp"), "tp"),
        P(("grp", "sp"), "tp"),
        P(("grp", "sp"), "tp"),
        P(("grp", "sp"), "tp"),
        P(("grp", "sp"), None),
        P("tp", None),
        P(),
        P(),
        P(),
        P("sp", "tp"),
        P("sp", "tp"),
        P("sp", "tp"),
    )
    return jax.shard_map(
        shards, mesh=mesh, in_specs=placed, out_specs=P(("grp", "sp"), None), check_vma=False
    )
```

profile of v0, /device:TPU:33, one launch (start us, length us, event | category | flops | bytes accessed | tf_op | source)
XLA Modules:
  0.0 380.9 jit_solution(10626614286702038167)
XLA Ops:
  6.6 0.8 copy.57
  7.4 1.4 pad_maximum_fusion.1
  8.9 1.7 pad_maximum_fusion
  10.8 142.7 %all-gather.5.cloned.1.call-done = bf16[4096,257]{1,0:T(8,128)(2,1)} async-done(((bf16[128,257]{1,0:T(8,128)(2,1)}), bf16[4096,257]{1,0:T(8,128)(2,1)}) %all-gather.5.cloned.1.call-update) | async-done | bytes 2105360 | tf_op jit(solution)/shard_map/all_gather | solution.py:12
  153.5 1.2 slice-done
  154.7 0.4 copy.58
  155.1 3.0 fusion.60
  158.2 0.2 broadcast_in_dim.14
  158.4 26.5 %while.13 = (s32[]{:T(128)}, f32[1,128,32]{1,2,0:T(8,128)S(1)}, f32[32,1,128,128]{3,2,0,1:T(8,128)S(1)}, s32[16]{0:T(128)S(1)}, s32[]{:T(128)}, /*index=5*/bf16[...) while((s32[]{:T(128)}, f32[1,128,32]{1,2,0:T(8,128)S(1)}, ...), condition=%wide.region_5.6_spmd.clone, body=%wide.region_0.5_spmd.clone.sunk | while | flops 22315912 | bytes 2536307 | solution.py:126
  158.4 0.6 dynamic_slice.40
  159.7 4.5 %conditional.3 = (f32[1,128,2]{1,2,0:T(2,128)S(1)}, f32[2,1,128,128]{3,2,0,1:T(8,128)S(1)}) conditional(s32[]{:T(128)} %convert_element_type.122, () %tuple.51, (s32[]{:T(128)}, s32[]{:T(128)}, s32[]{:T(128)}, bf16[4096,128]{1,0:T(8,128)(2,1)}, bf16[1,128,128]{2,1,0:T(8,128)(2,1)S(1)}, /*index=5*/bf16[4096,1]{0,1:T(2,128)(2,1)S(1)}, ...), branch_computations={%region_1.1_spmd, %region_2.4_spmd} | conditional | flops 22315908 | bytes 2271326 | solution.py:99
  160.4 1.0 fusion.2
  161.6 0.1 copy.55
  161.7 1.1 fusion.61
  162.8 0.1 copy.56
  162.9 0.9 constant_dynamic-slice_fusion
  163.8 0.3 convolution_bitcast_fusion
  164.1 0.1 fusion.6
  164.3 0.6 dynamic_slice.40
  165.6 0.6 dynamic_slice.40
  167.0 0.6 dynamic_slice.40
  168.4 0.6 dynamic_slice.40
  169.8 0.6 dynamic_slice.40
  171.1 0.6 dynamic_slice.40
  172.5 0.6 dynamic_slice.40
  173.9 0.6 dynamic_slice.40
  175.3 0.6 dynamic_slice.40
  176.7 0.6 dynamic_slice.40
  178.0 0.6 dynamic_slice.40
  179.4 0.6 dynamic_slice.40
  180.8 0.6 dynamic_slice.40
  182.2 0.6 dynamic_slice.40
  183.5 0.6 dynamic_slice.40
  185.0 0.1 copy.59
  185.1 2.9 fusion.28
  188.0 0.3 convolution_convert_fusion
  188.3 0.5 broadcast_in_dim.15
  188.8 73.7 %all_to_all.5 = bf16[8,128,2048]{2,1,0:T(8,128)(2,1)} all-to-all(bf16[8,128,2048]{2,1,0:T(8,128)(2,1)S(1)} %broadcast_in_dim.15), channel_id=1, replica_groups=mesh['grp'=2,'sp'=32,'tp'=8] {'tp'}, dimensions={0} | all-to-all | bytes 8388608 | tf_op jit(solution)/shard_map/all_to_all | solution.py:18
  262.6 3.0 reduce_sum.62
  265.6 0.2 fusion.38
  265.8 0.4 fusion.44
  266.3 31.7 %all-gather.7.cloned.1.call-done = bf16[2048,1920]{1,0:T(8,128)(2,1)} async-done(((bf16[64,1920]{1,0:T(8,128)(2,1)}), bf16[2048,1920]{1,0:T(8,128)(2,1)}) %all-gather.7.cloned.1.call-update) | async-done | bytes 7864336 | tf_op jit(solution)/shard_map/all_gather | solution.py:12
  298.0 2.4 fusion.23
  300.4 4.8 %fusion.25 = bf16[128,2048]{1,0:T(8,128)(2,1)} fusion(bf16[2048,1920]{1,0:T(8,128)(2,1)} %all-gather.7.cloned.1.call-done, f32[128,640]{1,0:T(8,128)S(1)} %fusion.23, bf16[128,2048]{1,0:T(8,128)(2,1)S(1)} %get-tuple-element.269, f32[128]{0:T(128)S(1)} %add_rsqrt_fusion.1, f32[2048]{0:T(1024)S(1)} %copy-done.5), kind=kOutput, calls=%fused_computation.36 | convolution fusion | flops 672890880 | bytes 6627840 | tf_op jit(solution)/shard_map/dot_general | solution.py:146
  305.2 64.9 %all-gather.9.cloned.1.call-done = bf16[1024,2048]{1,0:T(8,128)(2,1)} async-done(((bf16[128,2048]{1,0:T(8,128)(2,1)}), bf16[1024,2048]{1,0:T(8,128)(2,1)}) %all-gather.9.cloned.1.call-update) | async-done | bytes 4194320 | tf_op jit(solution)/shard_map/all_gather | solution.py:27
  370.1 3.0 reduce_sum.65
  373.1 0.2 fusion.42
  373.3 1.1 fusion.47
  (124 shorter events, 1.9 us)
Async XLA Ops:
  6.5 181.5 %copy-start = (bf16[128,2048]{1,0:T(8,128)(2,1)S(1)}, bf16[128,2048]{1,0:T(8,128)(2,1)}, u32[]{:S(2)}) copy-start(bf16[128,2048]{1,0:T(8,128)(2,1)} %param.21) | copy-start | bytes 1572868
  6.6 146.9 %all-gather.5.cloned.1.call-start = ((), (), s32[]{:S(2)}) async-start(), calls=%async_computation.1 | async-start | bytes 3244032 | tf_op jit(solution)/shard_map/all_gather | solution.py:12
  8.9 289.1 %all-gather.7.cloned.1.call-start = ((), (), s32[]{:S(2)}) async-start(), calls=%async_computation.2 | async-start | bytes 8110080 | tf_op jit(solution)/shard_map/all_gather | solution.py:12
  10.7 359.4 %all-gather.9.cloned.1.call-start = ((), (), s32[]{:S(2)}) async-start(), calls=%async_computation.3 | async-start | bytes 4718592 | tf_op jit(solution)/shard_map/all_gather | solution.py:27
  153.5 1.2 slice-start
  155.1 3.3 copy-start.1
  262.6 3.3 copy-start.2
  262.6 3.3 copy-start.3
  262.6 35.4 %copy-start.5 = (f32[2048]{0:T(1024)S(1)}, f32[2048]{0:T(1024)}, u32[]{:S(2)}) copy-start(f32[2048]{0:T(1024)} %param.23) | copy-start | bytes 24580
  370.1 3.2 copy-start.4
Sparse Core Ops, SparseCore 0:
  9.4 144.0 all-gather.4
  155.6 142.3 all-gather.6
  305.3 64.6 all-gather.8
where the time goes:
time: 383 us; the launch traced here: 381 us
  waiting for transfers between devices  239 us (62%)
  blocking collectives  73.7 us (19%)
  local copies, waits for them, and re-layouts  17.9 us (5%)
  between operations  13.3 us (3%)
  other arithmetic  12.4 us (3%)
  loops' own time  12.3 us (3%)
  matrix products  11.7 us (3%)
    all_gather x2, waiting for transfers between devices, sent_together(): result = lax.all_gather(both, axis, axis=dim, tiled=True)  174 us
    all_to_all x1, blocking collectives, sent_to_all(): lax.all_to_all(jnp.broadcast_to(x[None], (count, *x.shape)), axis, 0, 0,...  73.7 us
    all_gather x1, waiting for transfers between devices, total_of_pieces(): return lax.all_gather(x, axis).astype(jnp.float32).sum(0)  64.9 us
    another operation x1, loops' own time, shards(): lax.scan(one_group, tables, jnp.arange(shard_count // group_size, dtype=j...  11.1 us
    dynamic_slice x16, local copies, waits for them, and re-layouts, shards(): lax.scan(one_group, tables, jnp.arange(shard_count // group_size, dtype=j...  9.73 us
  transfers between devices with their start and end apart: 3, of which 3 were waited for; matrix products, arithmetic and copies ran while one was open for 7% of the time, Pallas kernels for 0%

commit v1 on v0

v1 whole, which is shorter than its diff:
```python
import functools

import jax
import jax.numpy as jnp
from jax import lax
from jax.experimental import pallas as pl
from jax.experimental.pallas import tpu as pltpu
from jax.sharding import PartitionSpec as P

EPSILON = 1e-06
MESH = pl.DeviceIdType.MESH
F32 = jnp.float32
BF16 = jnp.bfloat16
LAG = 12


def layer_kernel(
    sizes,
    q_ref,
    k_ref,
    v_ref,
    lg_ref,
    res_ref,
    ow_ref,
    mix_gain_ref,
    ffn_gain_ref,
    out_gain_ref,
    gate_ref,
    up_ref,
    down_ref,
    out_ref,
    kv_all,
    m_all,
    o_all,
    d_all,
    ow_all,
    att_all,
    mixed,
    middle,
    normed,
    m_act,
    o_act,
    hidden,
    parts,
    rs_buf,
    ffn,
    upper,
    acc_near,
    run_near,
    acc_far,
    local_sem,
    kv_send,
    kv_recv,
    m_send,
    m_recv,
    d_send,
    d_recv,
    y_send,
    y_recv,
    ow_send,
    ow_recv,
    ow_pass_send,
    ow_pass_recv,
    att_send,
    att_recv,
    rs_send,
    rs_recv,
    ag_send,
    ag_recv,
):
    n, t = sizes
    tok, width = q_ref.shape
    w_rows = gate_ref.shape[0]
    half_rows = w_rows // 2
    d_model = res_ref.shape[1]
    first_steps, second_steps = n // 2, n - 1 - n // 2
    lag = min(LAG, first_steps)
    tile = 128
    tile_pairs = d_model // tile // 2
    own_rows = tok // t
    grp, i, c = lax.axis_index("grp"), lax.axis_index("sp"), lax.axis_index("tp")
    parity = lax.rem(grp, 2)
    partner = grp + 1 - 2 * parity
    sibling = c + 1 - 2 * lax.rem(c, 2)
    right, left = lax.rem(i + 1, n), lax.rem(i + n - 1, n)

    def peer(k):
        return lax.rem(c + k, t)

    kv_own = kv_all.at[i]
    w_own = pl.ds(pl.multiple_of(i * w_rows, w_rows), w_rows)
    copies = [
        pltpu.make_async_copy(k_ref, kv_own.at[pl.ds(0, tok)], local_sem.at[0]),
        pltpu.make_async_copy(v_ref, kv_own.at[pl.ds(tok, tok)], local_sem.at[1]),
        pltpu.make_async_copy(lg_ref, kv_own.at[pl.ds(2 * tok, 16)], local_sem.at[2]),
        pltpu.make_async_copy(down_ref, d_all.at[w_own], local_sem.at[3]),
        pltpu.make_async_copy(
            ow_ref, ow_all.at[pl.ds(pl.multiple_of(c * width, width), width)], local_sem.at[4]
        ),
    ]
    for copy in copies:
        copy.start()

    @pl.when(parity == 0)
    def _():
        pltpu.make_async_copy(gate_ref, m_all.at[w_own], local_sem.at[5]).start()
        pltpu.make_async_copy(up_ref, o_all.at[w_own], local_sem.at[6]).start()

    @pl.when(parity == 1)
    def _():
        pltpu.make_async_copy(up_ref, m_all.at[w_own], local_sem.at[5]).start()
        pltpu.make_async_copy(gate_ref, o_all.at[w_own], local_sem.at[6]).start()

    barrier = pltpu.get_barrier_semaphore()
    for where in [{"sp": right}, {"sp": left}, {"grp": partner}] + [
        {"tp": peer(k)} for k in range(1, t)
    ]:
        pl.semaphore_signal(barrier, inc=1, device_id=where, device_id_type=MESH)

    rows = lax.broadcasted_iota(jnp.int32, (tile, 2 * tile), 0)
    cols = lax.broadcasted_iota(jnp.int32, (tile, 2 * tile), 1)
    upper[...] = jnp.where((rows > cols) | (cols >= tile), 1.0, 0.0).astype(BF16)
    acc_far[...] = jnp.zeros_like(acc_far)

    for copy in copies:
        copy.wait()
    pltpu.make_async_copy(gate_ref, m_all.at[w_own], local_sem.at[5]).wait()
    pltpu.make_async_copy(up_ref, o_all.at[w_own], local_sem.at[6]).wait()
    pl.semaphore_wait(barrier, t + 2)

    def block_at(direction, back):
        return lax.rem(i + n - back, n) if direction == 0 else lax.rem(i + back, n)

    def kv_copy(direction, step, back):
        block = kv_all.at[block_at(direction, back)]
        return pltpu.make_async_remote_copy(
            src_ref=block,
            dst_ref=block,
            send_sem=kv_send,
            recv_sem=kv_recv.at[direction, step - 1],
            device_id={"sp": right if direction == 0 else left},
            device_id_type=MESH,
        )

    def half_of(direction, back, half):
        start = block_at(direction, back) * w_rows + half * half_rows
        return pl.ds(pl.multiple_of(start, half_rows), half_rows)

    def w_copy(ref, send, recv, direction, step, back, half):
        part = ref.at[half_of(direction, back, half)]
        return pltpu.make_async_remote_copy(
            src_ref=part,
            dst_ref=part,
            send_sem=send,
            recv_sem=recv.at[direction, half, step - 1],
            device_id={"sp": right if direction == 0 else left},
            device_id_type=MESH,
        )

    def steps_of(direction, flipped):
        return first_steps if direction == int(flipped) else second_steps

    def if_step(condition, body):
        if isinstance(condition, bool):
            if condition:
                body()
        else:
            pl.when(condition)(body)

    def kv_slot(s):
        for direction in (0, 1):
            count = steps_of(direction, False)

            def arrived(direction=direction, count=count):
                kv_copy(direction, s, s).wait_recv()
                if_step(s < count, lambda: kv_copy(direction, s + 1, s).start())

            if_step(s <= count, arrived)

    def w_slot(ref, send, recv, s, flipped, to_partner):
        for half in (0, 1):
            for direction in (0, 1):
                count = steps_of(direction, flipped)

                def arrived(direction=direction, count=count, half=half):
                    w_copy(ref, send, recv, direction, s, s, half).wait_recv()
                    if_step(
                        s < count,
                        lambda: w_copy(ref, send, recv, direction, s + 1, s, half).start(),
                    )
                    if to_partner:
                        part = half_of(direction, s, half)
                        pltpu.make_async_remote_copy(
                            src_ref=m_all.at[part],
                            dst_ref=o_all.at[part],
                            send_sem=y_send,
                            recv_sem=y_recv,
                            device_id={"grp": partner},
                            device_id_type=MESH,
                        ).start()

                if_step(s <= count, arrived)

    def m_slot(s):
        w_slot(m_all, m_send, m_recv, s, True, True)

    def d_slot(s):
        w_slot(d_all, d_send, d_recv, s, False, False)

    def d_first():
        for half in (0, 1):
            for direction in (0, 1):
                w_copy(d_all, d_send, d_recv, direction, 1, 0, half).start()

    for direction in (0, 1):
        kv_copy(direction, 1, 0).start()
    for half in (0, 1):
        for direction in (0, 1):
            w_copy(m_all, m_send, m_recv, direction, 1, 0, half).start()

    def ow_block(index):
        return ow_all.at[pl.ds(pl.multiple_of(index * width, width), width)]

    def ow_copy(index, where, send, recv):
        return pltpu.make_async_remote_copy(
            src_ref=ow_block(index),
            dst_ref=ow_block(index),
            send_sem=send,
            recv_sem=recv,
            device_id={"tp": where},
            device_id_type=MESH,
        )

    for k in range(2, t, 2):
        ow_copy(c, peer(k), ow_send, ow_recv).start()
    ow_copy(c, sibling, ow_pass_send, ow_pass_recv).start()

    scale = width ** (-0.5)

    def terms(block, causal):
        k = kv_all[block, pl.ds(0, tok), :]
        v = kv_all[block, pl.ds(tok, tok), :]
        logit = kv_all[block, pl.ds(2 * tok, 16), :].astype(F32)[0:1, :]
        scores = lax.dot_general(
            q_ref[...], k, (((1,), (1,)), ((), ())), preferred_element_type=F32
        )
        scores = scores * scale + logit
        soft = jnp.log1p(jnp.exp(-jnp.abs(scores)))
        keep = -(jnp.maximum(scores, 0.0) + soft)
        if causal is not None:
            keep = jnp.where(causal, keep, 0.0)
        high = keep.astype(BF16)
        low = (keep - high.astype(F32)).astype(BF16)
        u = upper[...]
        sums = jnp.dot(high, u, preferred_element_type=F32) + jnp.dot(
            low, u, preferred_element_type=F32
        )
        within, total = sums[:, :tile], sums[:, tile:]
        stick = jnp.exp(jnp.minimum(scores, 0.0) - soft + within)
        if causal is not None:
            stick = jnp.where(causal, stick, 0.0)
        part = jnp.dot(stick.astype(BF16), v, preferred_element_type=F32)
        return total, part

    def attend(s):
        @pl.when(i >= s)
        def _():
            total, part = terms(i - s, None)
            so_far = run_near[...]
            acc_near[...] += jnp.exp(so_far) * part
            run_near[...] = so_far + total

        @pl.when((i + s >= n) & (s <= second_steps))
        def _():
            total, part = terms(i + s - n, None)
            acc_far[...] = acc_far[...] * jnp.exp(total) + part

    q_pos = lax.broadcasted_iota(jnp.int32, (tok, tok), 0)
    k_pos = lax.broadcasted_iota(jnp.int32, (tok, tok), 1)
    total, part = terms(i, k_pos < q_pos)
    acc_near[...] = part
    run_near[...] = total

    def early(s, carry):
        kv_slot(s)
        m_slot(s)
        attend(s)
        return carry

    def middle_slots(s, carry):
        kv_slot(s)
        m_slot(s)
        d_slot(s - lag)
        attend(s)
        return carry

    if lag > 0:
        lax.fori_loop(1, lag + 1, early, 0)
    d_first()
    if lag < first_steps:
        lax.fori_loop(lag + 1, first_steps + 1, middle_slots, 0)

    def columns(index, size):
        return pl.ds(pl.multiple_of(index * size, size), size)

    def send_attended():
        own = columns(c, width)
        att_all[:, own] = (acc_near[...] + jnp.exp(run_near[...]) * acc_far[...]).astype(BF16)
        if t > 2:
            x_rows = ow_all.at[pl.ds(0, (t // 2 - 1) * width)]
            pltpu.make_async_copy(x_rows, x_rows, ow_recv).wait()
            for k in range(2, t, 2):
                ow_copy(peer(k), sibling, ow_pass_send, ow_pass_recv).start()
        for k in range(1, t):
            pltpu.make_async_remote_copy(
                src_ref=att_all.at[:, own],
                dst_ref=att_all.at[:, own],
                send_sem=att_send,
                recv_sem=att_recv,
                device_id={"tp": peer(k)},
                device_id_type=MESH,
            ).start()

    wide = 256

    def wait_attended():
        others = att_all.at[:, pl.ds(0, (t - 1) * width)]
        pltpu.make_async_copy(others, others, att_recv).wait()
        passed = ow_all.at[pl.ds(0, (t // 2) * width)]
        pltpu.make_async_copy(passed, passed, ow_pass_recv).wait()

    def project():
        def step(j, carry):
            at = columns(j, wide)
            mixed[:, at] = jnp.dot(
                att_all[...], ow_all[:, at], preferred_element_type=F32
            ).astype(BF16)
            return carry

        lax.fori_loop(0, d_model // wide, step, 0)

    def normalize(x):
        return x * lax.rsqrt(jnp.mean(x * x, axis=-1, keepdims=True) + EPSILON)

    chunk = 16

    def norms():
        def step(j, carry):
            at = columns(j, chunk)
            mid = (
                res_ref[at, :].astype(F32)
                + mix_gain_ref[...] * normalize(mixed[at, :].astype(F32))
            ).astype(BF16)
            middle[at, :] = mid
            normed[at, :] = (ffn_gain_ref[...] * normalize(mid.astype(F32))).astype(BF16)
            return carry

        lax.fori_loop(0, tok // chunk, step, 0)

    def act_of(weights, act):
        act[...] = jnp.zeros_like(act)

        def step(j, carry):
            at = columns(j, wide)
            act[...] += jnp.dot(normed[:, at], weights[at, :], preferred_element_type=F32)
            return carry

        lax.fori_loop(0, d_model // wide, step, 0)

    def mine():
        act_of(m_all, m_act)

    def other():
        rest = o_all.at[pl.ds(0, (n - 1) * w_rows)]
        pltpu.make_async_copy(rest, rest, y_recv).wait()
        act_of(o_all, o_act)

    def hide():
        def step(j, carry):
            at = columns(j, chunk)
            a, b = m_act[at, :], o_act[at, :]
            gate = jnp.where(parity == 0, a, b)
            up = jnp.where(parity == 0, b, a)
            hidden[at, :] = (gate / (1.0 + jnp.exp(-gate)) * up).astype(BF16)
            return carry

        lax.fori_loop(0, tok // chunk, step, 0)

    count = d_model // tile
    own = pl.ds(pl.multiple_of(c * own_rows, own_rows), own_rows)

    def tiles_of(k):
        h, odd = i // 2, lax.rem(i, 2)
        return lax.rem(h - k + odd + count, count), lax.rem(h + k - 1 + odd, count)

    def partial_pair(k):
        for p in tiles_of(k):
            parts[p] = lax.dot_general(
                hidden[...],
                d_all[columns(p, tile), :],
                (((1,), (1,)), ((), ())),
                preferred_element_type=F32,
            ).astype(BF16)
            for far in range(1, t):
                rows_of = pl.ds(pl.multiple_of(peer(far) * own_rows, own_rows), own_rows)
                pltpu.make_async_remote_copy(
                    src_ref=parts.at[p, rows_of],
                    dst_ref=rs_buf.at[p, far - 1],
                    send_sem=rs_send,
                    recv_sem=rs_recv.at[p],
                    device_id={"tp": peer(far)},
                    device_id_type=MESH,
                ).start()

    def reduce_pair(k):
        for p in tiles_of(k):
            pltpu.make_async_copy(rs_buf.at[p], rs_buf.at[p], rs_recv.at[p]).wait()
            total = parts[p, own, :].astype(F32)
            for far in range(1, t):
                total = total + rs_buf[p, far - 1].astype(F32)
            ffn[p, own, :] = total.astype(BF16)
            for far in range(1, t):
                pltpu.make_async_remote_copy(
                    src_ref=ffn.at[p, own],
                    dst_ref=ffn.at[p, own],
                    send_sem=ag_send,
                    recv_sem=ag_recv.at[p],
                    device_id={"tp": peer(far)},
                    device_id_type=MESH,
                ).start()

    tasks = [
        send_attended,
        lambda: (wait_attended(), project()),
        norms,
        mine,
        other,
        hide,
    ]
    done_parts, done_sums = 0, 0

    def advance(ready, most):
        nonlocal done_parts, done_sums
        sums = done_parts
        for _ in range(most):
            if done_parts < ready:
                done_parts += 1
                partial_pair(done_parts)
        while done_sums < sums:
            done_sums += 1
            reduce_pair(done_sums)

    for s in range(first_steps - lag + 1, first_steps + 1):
        d_slot(s)
        if tasks:
            tasks.pop(0)()
        else:
            advance(s // 2, 2)
    while tasks:
        tasks.pop(0)()
    while done_sums < tile_pairs:
        advance(tile_pairs, tile_pairs)

    for p in range(count):
        others = rs_buf.at[p]
        pltpu.make_async_copy(others, others, ag_recv.at[p]).wait()

    def finish(j, carry):
        at = columns(j, chunk)
        x = jnp.concatenate([ffn[p, at, :] for p in range(count)], axis=1).astype(F32)
        out_ref[at, :] = (
            middle[at, :].astype(F32) + out_gain_ref[...] * normalize(x)
        ).astype(BF16)
        return carry

    lax.fori_loop(0, tok // chunk, finish, 0)

    def drain(ref, sem):
        pltpu.make_async_copy(ref, ref, sem).wait()

    drain(kv_all.at[pl.ds(0, n - 1)], kv_send)
    ring = pl.ds(0, (n - 1) * w_rows)
    drain(m_all.at[ring], m_send)
    drain(m_all.at[ring], y_send)
    drain(d_all.at[ring], d_send)
    if t > 2:
        drain(ow_all.at[pl.ds(0, (t // 2 - 1) * width)], ow_send)
    drain(ow_all.at[pl.ds(0, (t // 2) * width)], ow_pass_send)
    drain(att_all.at[:, pl.ds(0, (t - 1) * width)], att_send)
    drain(rs_buf, rs_send)
    drain(rs_buf, ag_send)


def solution(mesh):
    n, t = mesh.shape["sp"], mesh.shape["tp"]

    def shards(
        query_rows,
        key_rows,
        value_rows,
        key_logit,
        residual,
        out_weight,
        mix_gain,
        ffn_gain,
        out_gain,
        gate_weight,
        up_weight,
        down_weight,
    ):
        tok, width = query_rows.shape
        w_rows, units = gate_weight.shape
        d_model = residual.shape[1]
        tile = 128
        count = d_model // tile
        logit = jnp.broadcast_to(key_logit.reshape(1, tok), (16, tok))
        vmem = pl.BlockSpec(memory_space=pltpu.VMEM)
        anywhere = pl.BlockSpec(memory_space=pl.ANY)
        steps = n // 2
        dma = pltpu.SemaphoreType.DMA
        return pl.pallas_call(
            functools.partial(layer_kernel, (n, t)),
            out_shape=jax.ShapeDtypeStruct((tok, d_model), BF16),
            in_specs=[vmem] + [anywhere] * 3 + [vmem, anywhere] + [vmem] * 3 + [anywhere] * 3,
            out_specs=vmem,
            scratch_shapes=[
                pltpu.VMEM((n, 2 * tok + 16, width), BF16),
                pltpu.VMEM((n * w_rows, units), BF16),
                pltpu.VMEM((n * w_rows, units), BF16),
                pltpu.VMEM((n * w_rows, units), BF16),
                pltpu.VMEM((t * width, d_model), BF16),
                pltpu.VMEM((tok, t * width), BF16),
                pltpu.VMEM((tok, d_model), BF16),
                pltpu.VMEM((tok, d_model), BF16),
                pltpu.VMEM((tok, d_model), BF16),
                pltpu.VMEM((tok, units), F32),
                pltpu.VMEM((tok, units), F32),
                pltpu.VMEM((tok, units), BF16),
                pltpu.VMEM((count, tok, tile), BF16),
                pltpu.VMEM((count, t - 1, tok // t, tile), BF16),
                pltpu.VMEM((count, tok, tile), BF16),
                pltpu.VMEM((tile, 2 * tile), BF16),
                pltpu.VMEM((tok, width), F32),
                pltpu.VMEM((tok, width), F32),
                pltpu.VMEM((tok, width), F32),
                dma((7,)),
                dma,
                dma((2, steps)),
                dma,
                dma((2, 2, steps)),
                dma,
                dma((2, 2, steps)),
                dma,
                dma,
                dma,
                dma,
                dma,
                dma,
                dma,
                dma,
                dma,
                dma((count,)),
                dma,
                dma((count,)),
            ],
            compiler_params=pltpu.CompilerParams(
                collective_id=0, has_side_effects=True, vmem_limit_bytes=48 * 1024 * 1024
            ),
            name="layer",
        )(
            query_rows,
            key_rows,
            value_rows,
            logit,
            residual,
            out_weight,
            mix_gain.reshape(1, d_model),
            ffn_gain.reshape(1, d_model),
            out_gain.reshape(1, d_model),
            gate_weight,
            up_weight,
            down_weight,
        )

    rows = P(("grp", "sp"), "tp")
    placed = (
        rows,
        rows,
        rows,
        rows,
        P(("grp", "sp"), None),
        P("tp", None),
        P(),
        P(),
        P(),
        P("sp", "tp"),
        P("sp", "tp"),
        P("sp", "tp"),
    )
    return jax.shard_map(
        shards, mesh=mesh, in_specs=placed, out_specs=P(("grp", "sp"), None), check_vma=False
    )
```

time: 383 us -> 176 us (0.46)
  waiting for transfers between devices: 239 us -> 0 us
  Pallas kernels: 0 us -> 165 us
  blocking collectives: 73.7 us -> 0 us
  between operations: 13.3 us -> 0.02 us
  other arithmetic: 12.4 us -> 0 us
  loops' own time: 12.3 us -> 0 us
  matrix products: 11.7 us -> 0 us
  local copies, waits for them, and re-layouts: 17.9 us -> 9.9 us
    all_gather x3 -> x0, waiting for transfers between devices: 239 us -> none  [the longest x2 174 us: sent_together(): result = lax.all_gather(both, axis, axis=dim, tiled=True)]
    pallas_call x0 -> x1, Pallas kernels: none -> 165 us  [shards(): pl.pallas_call(functools.partial(layer_kernel, (n, t)), out_shape=jax.Sha...]
    all_to_all x1 -> x0, blocking collectives: 73.7 us -> none  [sent_to_all(): lax.all_to_all(jnp.broadcast_to(x[None], (count, *x.shape)), axis, 0, 0,...]
    another operation x17 -> x0, loops' own time: 12.3 us -> none  [the longest x1 11.1 us: shards(): lax.scan(one_group, tables, jnp.arange(shard_count // group_size, dtype=j...]
    dot_general x6 -> x0, matrix products: 11.7 us -> none  [the longest x1 4.8 us: shards(): lax.dot_general(hidden, whole_down, (((1,), (1,)), ((), ())), preferred_e...]
    dynamic_slice x17 -> x0, local copies, waits for them, and re-layouts: 10.6 us -> none  [the longest x16 9.73 us: shards(): lax.scan(one_group, tables, jnp.arange(shard_count // group_size, dtype=j...]
    unnamed x14 -> x23, local copies, waits for them, and re-layouts: 1.24 us -> 9.23 us
    reduce_sum x6 -> x0, other arithmetic: 6.91 us -> none  [the longest x1 3.04 us: over_copies(): return jnp.sum(everything.astype(jnp.float32), axis=0)]
  transfers between devices with their start and end apart: 3 -> 0, of which waited for: 3 -> 0; matrix products, arithmetic and copies ran while one was open for 7% -> 0% of each run, Pallas kernels for 0% -> 0%
where the time goes in v1:
time: 176 us; the launch traced here: 175 us
  Pallas kernels  165 us (94%)
  local copies, waits for them, and re-layouts  9.9 us (6%)
    pallas_call x1, Pallas kernels, shards(): pl.pallas_call(functools.partial(layer_kernel, (n, t)), out_shape=jax.Sha...  165 us
    unnamed x23, local copies, waits for them, and re-layouts  9.23 us

profile of v1, /device:TPU:33, one launch (start us, length us, event | category | flops | bytes accessed | tf_op | source)
XLA Modules:
  0.0 175.3 jit_solution(11766222111093196048)
XLA Ops:
  0.0 0.0 copy-start.8
  0.0 0.7 broadcast_in_dim.8.lg_ref
  0.7 0.0 copy-done.8
  0.7 0.0 copy-start
  0.7 1.0 copy-done
  1.7 0.0 copy-start.1
  1.7 1.0 copy-done.1
  2.8 0.0 copy-start.2
  2.8 0.9 copy-done.2
  3.7 0.0 copy-start.3
  3.7 0.9 copy-done.3
  4.6 0.0 copy-start.4
  4.6 0.9 copy-done.4
  5.4 0.0 copy-start.5
  5.4 0.8 copy-done.5
  6.2 0.0 copy-start.6
  6.2 0.8 copy-done.6
  7.0 0.0 copy-start.7
  7.0 0.8 copy-done.7
  7.7 0.0 copy-start.9
  7.7 0.7 copy-done.9
  8.4 0.0 copy-start.10
  8.4 0.7 copy-done.10
  9.1 165.3 %layer.1 = bf16[128,2048]{1,0:T(8,128)(2,1)S(1)} custom-call(bf16[128,128]{1,0:T(8,128)(2,1)S(1)} %copy-done.5, bf16[128,128]{1,0:T(8,128)(2,1)S(1)} %copy-done.6, bf16[128,128]{1,0:T(8,128)(2,1)S(1)} %copy-done.7, bf16[16,128]{1,0:T(8,128)(2,1)S(1)} %broadcast_in_dim.8.lg_ref, bf16[128,2048]{1,0:T(8,128)(2,1)S(1)} %copy-done, ...), custom_call_target="tpu_custom_call" | custom-call | tf_op jit(solution)/shard_map/layer/pallas_call | solution.py:521
  174.5 0.8 copy.14
Async XLA Ops:
  0.0 0.7 copy-start.8
  0.7 1.0 copy-start
  1.7 1.0 copy-start.1
  2.8 0.9 copy-start.2
  3.7 0.9 copy-start.3
  4.6 0.9 copy-start.4
  5.4 0.8 copy-start.5
  6.2 0.8 copy-start.6
  7.0 0.8 copy-start.7
  7.7 0.7 copy-start.9
  8.4 0.7 copy-start.10

commit v2 on v1

--- a/solution.py
+++ b/solution.py
@@ -11,24 +11,29 @@
 MESH = pl.DeviceIdType.MESH
 F32 = jnp.float32
 BF16 = jnp.bfloat16
-LAG = 12
+WIDE = 256
 
 
 def layer_kernel(
     sizes,
-    q_ref,
+    q_in,
     k_ref,
     v_ref,
     lg_ref,
-    res_ref,
+    res_in,
     ow_ref,
-    mix_gain_ref,
-    ffn_gain_ref,
-    out_gain_ref,
+    mix_gain_in,
+    ffn_gain_in,
+    out_gain_in,
     gate_ref,
     up_ref,
     down_ref,
     out_ref,
+    q_ref,
+    res_ref,
+    mix_gain_ref,
+    ffn_gain_ref,
+    out_gain_ref,
     kv_all,
     m_all,
     o_all,
@@ -69,14 +74,12 @@
     ag_recv,
 ):
     n, t = sizes
-    tok, width = q_ref.shape
+    tok, width = q_in.shape
     w_rows = gate_ref.shape[0]
     half_rows = w_rows // 2
     d_model = res_ref.shape[1]
     first_steps, second_steps = n // 2, n - 1 - n // 2
-    lag = min(LAG, first_steps)
-    tile = 128
-    tile_pairs = d_model // tile // 2
+    tile, wide = 128, WIDE
     own_rows = tok // t
     grp, i, c = lax.axis_index("grp"), lax.axis_index("sp"), lax.axis_index("tp")
     parity = lax.rem(grp, 2)
@@ -97,6 +100,11 @@
         pltpu.make_async_copy(
             ow_ref, ow_all.at[pl.ds(pl.multiple_of(c * width, width), width)], local_sem.at[4]
         ),
+        pltpu.make_async_copy(q_in, q_ref, local_sem.at[7]),
+        pltpu.make_async_copy(res_in, res_ref, local_sem.at[8]),
+        pltpu.make_async_copy(mix_gain_in, mix_gain_ref, local_sem.at[9]),
+        pltpu.make_async_copy(ffn_gain_in, ffn_gain_ref, local_sem.at[10]),
+        pltpu.make_async_copy(out_gain_in, out_gain_ref, local_sem.at[11]),
     ]
     for copy in copies:
         copy.start()
@@ -122,11 +130,13 @@
     upper[...] = jnp.where((rows > cols) | (cols >= tile), 1.0, 0.0).astype(BF16)
     acc_far[...] = jnp.zeros_like(acc_far)
 
-    for copy in copies:
-        copy.wait()
-    pltpu.make_async_copy(gate_ref, m_all.at[w_own], local_sem.at[5]).wait()
-    pltpu.make_async_copy(up_ref, o_all.at[w_own], local_sem.at[6]).wait()
-    pl.semaphore_wait(barrier, t + 2)
+    with jax.named_scope("local"):
+        for copy in copies:
+            copy.wait()
+        pltpu.make_async_copy(gate_ref, m_all.at[w_own], local_sem.at[5]).wait()
+        pltpu.make_async_copy(up_ref, o_all.at[w_own], local_sem.at[6]).wait()
+    with jax.named_scope("barrier"):
+        pl.semaphore_wait(barrier, t + 2)
 
     def block_at(direction, back):
         return lax.rem(i + n - back, n) if direction == 0 else lax.rem(i + back, n)
@@ -177,46 +187,43 @@
 
             if_step(s <= count, arrived)
 
-    def w_slot(ref, send, recv, s, flipped, to_partner):
-        for half in (0, 1):
-            for direction in (0, 1):
-                count = steps_of(direction, flipped)
-
-                def arrived(direction=direction, count=count, half=half):
-                    w_copy(ref, send, recv, direction, s, s, half).wait_recv()
-                    if_step(
-                        s < count,
-                        lambda: w_copy(ref, send, recv, direction, s + 1, s, half).start(),
-                    )
-                    if to_partner:
-                        part = half_of(direction, s, half)
-                        pltpu.make_async_remote_copy(
-                            src_ref=m_all.at[part],
-                            dst_ref=o_all.at[part],
-                            send_sem=y_send,
-                            recv_sem=y_recv,
-                            device_id={"grp": partner},
-                            device_id_type=MESH,
-                        ).start()
-
-                if_step(s <= count, arrived)
-
-    def m_slot(s):
-        w_slot(m_all, m_send, m_recv, s, True, True)
-
-    def d_slot(s):
-        w_slot(d_all, d_send, d_recv, s, False, False)
-
-    def d_first():
-        for half in (0, 1):
-            for direction in (0, 1):
-                w_copy(d_all, d_send, d_recv, direction, 1, 0, half).start()
+    def w_arrived(ref, send, recv, s, half, direction, count):
+        w_copy(ref, send, recv, direction, s, s, half).wait_recv()
+        if_step(s < count, lambda: w_copy(ref, send, recv, direction, s + 1, s, half).start())
+
+    def to_partner(s, half, direction):
+        part = m_all.at[half_of(direction, s, half)]
+        pltpu.make_async_remote_copy(
+            src_ref=part,
+            dst_ref=o_all.at[half_of(direction, s, half)],
+            send_sem=y_send,
+            recv_sem=y_recv.at[s - 1],
+            device_id={"grp": partner},
+            device_id_type=MESH,
+        ).start()
+
+    def w_slot(s, half):
+        for direction in (0, 1):
+
+            def m_arrived(direction=direction, count=steps_of(direction, True)):
+                w_arrived(m_all, m_send, m_recv, s, half, direction, count)
+                to_partner(s, half, direction)
+
+            if_step(s <= steps_of(direction, True), m_arrived)
+        for direction in (0, 1):
+
+            def d_arrived(direction=direction, count=steps_of(direction, False)):
+                w_arrived(d_all, d_send, d_recv, s, half, direction, count)
+
+            if_step(s <= steps_of(direction, False), d_arrived)
 
     for direction in (0, 1):
         kv_copy(direction, 1, 0).start()
     for half in (0, 1):
         for direction in (0, 1):
             w_copy(m_all, m_send, m_recv, direction, 1, 0, half).start()
+        for direction in (0, 1):
+            w_copy(d_all, d_send, d_recv, direction, 1, 0, half).start()
 
     def ow_block(index):
         return ow_all.at[pl.ds(pl.multiple_of(index * width, width), width)]
@@ -262,7 +269,7 @@
         part = jnp.dot(stick.astype(BF16), v, preferred_element_type=F32)
         return total, part
 
-    def attend(s):
+    def attend_near(s):
         @pl.when(i >= s)
         def _():
             total, part = terms(i - s, None)
@@ -270,6 +277,7 @@
             acc_near[...] += jnp.exp(so_far) * part
             run_near[...] = so_far + total
 
+    def attend_far(s):
         @pl.when((i + s >= n) & (s <= second_steps))
         def _():
             total, part = terms(i + s - n, None)
@@ -281,24 +289,41 @@
     acc_near[...] = part
     run_near[...] = total
 
-    def early(s, carry):
-        kv_slot(s)
-        m_slot(s)
-        attend(s)
+    def group(g, carry):
+        s, w = 4 * g, 3 * g
+        with jax.named_scope("kv1"):
+            kv_slot(s + 1)
+        attend_near(s + 1)
+        with jax.named_scope("w1a"):
+            w_slot(w + 1, 0)
+        attend_far(s + 1)
+        with jax.named_scope("w1b"):
+            w_slot(w + 1, 1)
+        with jax.named_scope("kv2"):
+            kv_slot(s + 2)
+        attend_near(s + 2)
+        with jax.named_scope("w2a"):
+            w_slot(w + 2, 0)
+        attend_far(s + 2)
+        with jax.named_scope("kv3"):
+            kv_slot(s + 3)
+        attend_near(s + 3)
+        with jax.named_scope("w2b"):
+            w_slot(w + 2, 1)
+        attend_far(s + 3)
+        with jax.named_scope("w3a"):
+            w_slot(w + 3, 0)
+        with jax.named_scope("kv4"):
+            kv_slot(s + 4)
+        attend_near(s + 4)
+        with jax.named_scope("w3b"):
+            w_slot(w + 3, 1)
+        attend_far(s + 4)
         return carry
 
-    def middle_slots(s, carry):
-        kv_slot(s)
-        m_slot(s)
-        d_slot(s - lag)
-        attend(s)
-        return carry
-
-    if lag > 0:
-        lax.fori_loop(1, lag + 1, early, 0)
-    d_first()
-    if lag < first_steps:
-        lax.fori_loop(lag + 1, first_steps + 1, middle_slots, 0)
+    groups = first_steps // 4
+    early = 3 * groups
+    lax.fori_loop(0, groups, group, 0)
 
     def columns(index, size):
         return pl.ds(pl.multiple_of(index * size, size), size)
@@ -321,7 +346,6 @@
                 device_id_type=MESH,
             ).start()
 
-    wide = 256
 
     def wait_attended():
         others = att_all.at[:, pl.ds(0, (t - 1) * width)]
@@ -329,7 +353,7 @@
         passed = ow_all.at[pl.ds(0, (t // 2) * width)]
         pltpu.make_async_copy(passed, passed, ow_pass_recv).wait()
 
-    def project():
+    def project(start, stop):
         def step(j, carry):
             at = columns(j, wide)
             mixed[:, at] = jnp.dot(
@@ -337,14 +361,14 @@
             ).astype(BF16)
             return carry
 
-        lax.fori_loop(0, d_model // wide, step, 0)
+        lax.fori_loop(start, stop, step, 0)
 
     def normalize(x):
         return x * lax.rsqrt(jnp.mean(x * x, axis=-1, keepdims=True) + EPSILON)
 
     chunk = 16
 
-    def norms():
+    def norms(start, stop):
         def step(j, carry):
             at = columns(j, chunk)
             mid = (
@@ -355,25 +379,25 @@
             normed[at, :] = (ffn_gain_ref[...] * normalize(mid.astype(F32))).astype(BF16)
             return carry
 
-        lax.fori_loop(0, tok // chunk, step, 0)
-
-    def act_of(weights, act):
-        act[...] = jnp.zeros_like(act)
-
+        lax.fori_loop(start, stop, step, 0)
+
+    chunks, per_chunk = d_model // wide, wide // w_rows
+    arrived_chunks = max(0, min(chunks, (2 * early + 2 - per_chunk) // per_chunk))
+    first_chunk = (i + n - early + per_chunk - 1) // per_chunk
+
+    def act_of(weights, act, start, stop):
         def step(j, carry):
-            at = columns(j, wide)
+            at = columns(lax.rem(first_chunk + j, chunks), wide)
             act[...] += jnp.dot(normed[:, at], weights[at, :], preferred_element_type=F32)
             return carry
 
-        lax.fori_loop(0, d_model // wide, step, 0)
-
-    def mine():
-        act_of(m_all, m_act)
-
-    def other():
-        rest = o_all.at[pl.ds(0, (n - 1) * w_rows)]
-        pltpu.make_async_copy(rest, rest, y_recv).wait()
-        act_of(o_all, o_act)
+        lax.fori_loop(start, stop, step, 0)
+
+    def wait_other(start, stop):
+        for s in range(start, stop):
+            blocks = int(s <= first_steps) + int(s <= second_steps)
+            rest = o_all.at[pl.ds(0, blocks * w_rows)]
+            pltpu.make_async_copy(rest, rest, y_recv.at[s - 1]).wait()
 
     def hide():
         def step(j, carry):
@@ -386,84 +410,100 @@
 
         lax.fori_loop(0, tok // chunk, step, 0)
 
-    count = d_model // tile
+    count = d_model // wide
     own = pl.ds(pl.multiple_of(c * own_rows, own_rows), own_rows)
 
-    def tiles_of(k):
-        h, odd = i // 2, lax.rem(i, 2)
-        return lax.rem(h - k + odd + count, count), lax.rem(h + k - 1 + odd, count)
-
-    def partial_pair(k):
-        for p in tiles_of(k):
-            parts[p] = lax.dot_general(
-                hidden[...],
-                d_all[columns(p, tile), :],
-                (((1,), (1,)), ((), ())),
-                preferred_element_type=F32,
-            ).astype(BF16)
-            for far in range(1, t):
-                rows_of = pl.ds(pl.multiple_of(peer(far) * own_rows, own_rows), own_rows)
-                pltpu.make_async_remote_copy(
-                    src_ref=parts.at[p, rows_of],
-                    dst_ref=rs_buf.at[p, far - 1],
-                    send_sem=rs_send,
-                    recv_sem=rs_recv.at[p],
-                    device_id={"tp": peer(far)},
-                    device_id_type=MESH,
-                ).start()
-
-    def reduce_pair(k):
-        for p in tiles_of(k):
-            pltpu.make_async_copy(rs_buf.at[p], rs_buf.at[p], rs_recv.at[p]).wait()
-            total = parts[p, own, :].astype(F32)
-            for far in range(1, t):
-                total = total + rs_buf[p, far - 1].astype(F32)
-            ffn[p, own, :] = total.astype(BF16)
-            for far in range(1, t):
-                pltpu.make_async_remote_copy(
-                    src_ref=ffn.at[p, own],
-                    dst_ref=ffn.at[p, own],
-                    send_sem=ag_send,
-                    recv_sem=ag_recv.at[p],
-                    device_id={"tp": peer(far)},
-                    device_id_type=MESH,
-                ).start()
+    def partial(p, carry):
+        parts[p] = lax.dot_general(
+            hidden[...],
+            d_all[columns(p, wide), :],
+            (((1,), (1,)), ((), ())),
+            preferred_element_type=F32,
+        ).astype(BF16)
+        for far in range(1, t):
+            rows_of = pl.ds(pl.multiple_of(peer(far) * own_rows, own_rows), own_rows)
+            pltpu.make_async_remote_copy(
+                src_ref=parts.at[p, rows_of],
+                dst_ref=rs_buf.at[p, far - 1],
+                send_sem=rs_send,
+                recv_sem=rs_recv.at[p],
+                device_id={"tp": peer(far)},
+                device_id_type=MESH,
+            ).start()
+        return carry
+
+    def total_of(p, carry):
+        pltpu.make_async_copy(rs_buf.at[p], rs_buf.at[p], rs_recv.at[p]).wait()
+        total = parts[p, own, :].astype(F32)
+        for far in range(1, t):
+            total = total + rs_buf[p, far - 1].astype(F32)
+        ffn[p, own, :] = total.astype(BF16)
+        for far in range(1, t):
+            pltpu.make_async_remote_copy(
+                src_ref=ffn.at[p, own],
+                dst_ref=ffn.at[p, own],
+                send_sem=ag_send,
+                recv_sem=ag_recv.at[p],
+                device_id={"tp": peer(far)},
+                device_id_type=MESH,
+            ).start()
+        return carry
+
+    def zero_acts():
+        m_act[...] = jnp.zeros_like(m_act)
+        o_act[...] = jnp.zeros_like(o_act)
+
+    n_cols, n_rows = d_model // wide, tok // chunk
+    some = arrived_chunks // 2
+
+    def named(name, *bodies):
+        def run():
+            with jax.named_scope(name):
+                for body in bodies:
+                    body()
+
+        return run
 
     tasks = [
-        send_attended,
-        lambda: (wait_attended(), project()),
-        norms,
-        mine,
-        other,
-        hide,
+        named("zero", zero_acts),
+        named("project1", wait_attended, lambda: project(0, n_cols // 2)),
+        named("project2", lambda: project(n_cols // 2, n_cols)),
+        named("norms1", lambda: norms(0, n_rows // 2)),
+        named("norms2", lambda: norms(n_rows // 2, n_rows)),
+        named("mine1", lambda: act_of(m_all, m_act, 0, some)),
+        named("mine2", lambda: act_of(m_all, m_act, some, arrived_chunks)),
+        named(
+            "other1",
+            lambda: wait_other(1, early + 1),
+            lambda: act_of(o_all, o_act, 0, arrived_chunks),
+        ),
     ]
-    done_parts, done_sums = 0, 0
-
-    def advance(ready, most):
-        nonlocal done_parts, done_sums
-        sums = done_parts
-        for _ in range(most):
-            if done_parts < ready:
-                done_parts += 1
-                partial_pair(done_parts)
-        while done_sums < sums:
-            done_sums += 1
-            reduce_pair(done_sums)
-
-    for s in range(first_steps - lag + 1, first_steps + 1):
-        d_slot(s)
-        if tasks:
-            tasks.pop(0)()
-        else:
-            advance(s // 2, 2)
+    with jax.named_scope("send_attended"):
+        send_attended()
+    for s in range(early + 1, first_steps + 1):
+        for half in (0, 1):
+            with jax.named_scope("wl"):
+                w_slot(s, half)
+            if tasks:
+                tasks.pop(0)()
     while tasks:
         tasks.pop(0)()
-    while done_sums < tile_pairs:
-        advance(tile_pairs, tile_pairs)
-
-    for p in range(count):
-        others = rs_buf.at[p]
-        pltpu.make_async_copy(others, others, ag_recv.at[p]).wait()
+    with jax.named_scope("mine3"):
+        act_of(m_all, m_act, arrived_chunks, chunks)
+    with jax.named_scope("other2"):
+        wait_other(early + 1, first_steps + 1)
+        act_of(o_all, o_act, arrived_chunks, chunks)
+    with jax.named_scope("hide"):
+        hide()
+    with jax.named_scope("partial"):
+        lax.fori_loop(0, count, partial, 0)
+    with jax.named_scope("total"):
+        lax.fori_loop(0, count, total_of, 0)
+
+    with jax.named_scope("gathered"):
+        for p in range(count):
+            others = rs_buf.at[p]
+            pltpu.make_async_copy(others, others, ag_recv.at[p]).wait()
 
     def finish(j, carry):
         at = columns(j, chunk)
@@ -473,7 +513,8 @@
         ).astype(BF16)
         return carry
 
-    lax.fori_loop(0, tok // chunk, finish, 0)
+    with jax.named_scope("finish"):
+        lax.fori_loop(0, tok // chunk, finish, 0)
 
     def drain(ref, sem):
         pltpu.make_async_copy(ref, ref, sem).wait()
@@ -512,18 +553,23 @@
         w_rows, units = gate_weight.shape
         d_model = residual.shape[1]
         tile = 128
-        count = d_model // tile
+        count = d_model // WIDE
         logit = jnp.broadcast_to(key_logit.reshape(1, tok), (16, tok))
         vmem = pl.BlockSpec(memory_space=pltpu.VMEM)
-        anywhere = pl.BlockSpec(memory_space=pl.ANY)
+        hbm = pl.BlockSpec(memory_space=pltpu.HBM)
         steps = n // 2
         dma = pltpu.SemaphoreType.DMA
         return pl.pallas_call(
             functools.partial(layer_kernel, (n, t)),
             out_shape=jax.ShapeDtypeStruct((tok, d_model), BF16),
-            in_specs=[vmem] + [anywhere] * 3 + [vmem, anywhere] + [vmem] * 3 + [anywhere] * 3,
+            in_specs=[hbm] * 12,
             out_specs=vmem,
             scratch_shapes=[
+                pltpu.VMEM((tok, width), BF16),
+                pltpu.VMEM((tok, d_model), BF16),
+                pltpu.VMEM((1, d_model), F32),
+                pltpu.VMEM((1, d_model), F32),
+                pltpu.VMEM((1, d_model), F32),
                 pltpu.VMEM((n, 2 * tok + 16, width), BF16),
                 pltpu.VMEM((n * w_rows, units), BF16),
                 pltpu.VMEM((n * w_rows, units), BF16),
@@ -536,14 +582,14 @@
                 pltpu.VMEM((tok, units), F32),
                 pltpu.VMEM((tok, units), F32),
                 pltpu.VMEM((tok, units), BF16),
-                pltpu.VMEM((count, tok, tile), BF16),
-                pltpu.VMEM((count, t - 1, tok // t, tile), BF16),
-                pltpu.VMEM((count, tok, tile), BF16),
+                pltpu.VMEM((count, tok, WIDE), BF16),
+                pltpu.VMEM((count, t - 1, tok // t, WIDE), BF16),
+                pltpu.VMEM((count, tok, WIDE), BF16),
                 pltpu.VMEM((tile, 2 * tile), BF16),
                 pltpu.VMEM((tok, width), F32),
                 pltpu.VMEM((tok, width), F32),
                 pltpu.VMEM((tok, width), F32),
-                dma((7,)),
+                dma((12,)),
                 dma,
                 dma((2, steps)),
                 dma,
@@ -551,7 +597,7 @@
                 dma,
                 dma((2, 2, steps)),
                 dma,
-                dma,
+                dma((steps,)),
                 dma,
                 dma,
                 dma,
@@ -564,7 +610,7 @@
                 dma((count,)),
             ],
             compiler_params=pltpu.CompilerParams(
-                collective_id=0, has_side_effects=True, vmem_limit_bytes=48 * 1024 * 1024
+                collective_id=0, has_side_effects=True, vmem_limit_bytes=67043328
             ),
             name="layer",
         )(

time: 176 us -> 157 us (0.89)
  Pallas kernels: 165 us -> 154 us
  local copies, waits for them, and re-layouts: 9.9 us -> 3.13 us
    pallas_call x1, Pallas kernels: 165 us -> 154 us  [shards(): pl.pallas_call(functools.partial(layer_kernel, (n, t)), out_shape=jax.Sha...]
    unnamed x23 -> x3, local copies, waits for them, and re-layouts: 9.23 us -> 2.54 us
where the time goes in v2:
time: 157 us
  Pallas kernels  154 us (98%)
  local copies, waits for them, and re-layouts  3.13 us (2%)
    pallas_call x1, Pallas kernels, shards(): pl.pallas_call(functools.partial(layer_kernel, (n, t)), out_shape=jax.Sha...  154 us

profile of v2, /device:TPU:33, one launch (start us, length us, event | category | flops | bytes accessed | tf_op | source)
XLA Modules:
  0.0 156.8 jit_solution(781100457326727105)
XLA Ops:
  0.0 0.0 copy-start
  0.0 0.7 copy-done
  0.7 0.6 broadcast_in_dim.8.lg_ref
  1.3 153.7 %layer.1 = bf16[128,2048]{1,0:T(8,128)(2,1)} custom-call(bf16[128,128]{1,0:T(8,128)(2,1)} %q_in.1, bf16[128,128]{1,0:T(8,128)(2,1)} %k_ref.1, bf16[128,128]{1,0:T(8,128)(2,1)} %v_ref.1, bf16[16,128]{1,0:T(8,128)(2,1)} %broadcast_in_dim.8.lg_ref, bf16[128,2048]{1,0:T(8,128)(2,1)} %res_in.1, bf16[128,2048]{1,0:T(8,128)(2,1)} %ow_ref.1, f32[1,2048]{1,0:T(1,128)} %bitcast.4, ...), custom_call_target="tpu_custom_call" | custom-call | tf_op jit(solution)/shard_map/layer/pallas_call | solution.py:562
  154.9 1.9 %copy.14 = bf16[128,2048]{1,0:T(8,128)(2,1)} copy(bf16[128,2048]{1,0:T(8,128)(2,1)} %layer.1) | data formatting | bytes 1048576
Async XLA Ops:
  0.0 0.7 copy-start

commit v3 on v2

--- a/solution.py
+++ b/solution.py
@@ -12,6 +12,8 @@
 F32 = jnp.float32
 BF16 = jnp.bfloat16
 WIDE = 256
+LAST = 2
+BEHIND = 3
 
 
 def layer_kernel(
@@ -47,6 +49,8 @@
     o_act,
     hidden,
     parts,
+    core_buf,
+    halves,
     rs_buf,
     ffn,
     upper,
@@ -72,6 +76,19 @@
     rs_recv,
     ag_send,
     ag_recv,
+    cs_send,
+    cs_recv,
+    cg_send,
+    cg_recv,
+    dy_send,
+    dy_recv,
+    out,
+    out_sem,
+    rs_last,
+    ls_send,
+    ls_recv,
+    lg_send,
+    lg_recv,
 ):
     n, t = sizes
     tok, width = q_in.shape
@@ -141,13 +158,14 @@
     def block_at(direction, back):
         return lax.rem(i + n - back, n) if direction == 0 else lax.rem(i + back, n)
 
-    def kv_copy(direction, step, back):
-        block = kv_all.at[block_at(direction, back)]
+    def kv_copy(direction, step, back, part):
+        rows_of = pl.ds(0, tok) if part == 0 else pl.ds(tok, tok + 16)
+        block = kv_all.at[block_at(direction, back), rows_of]
         return pltpu.make_async_remote_copy(
             src_ref=block,
             dst_ref=block,
-            send_sem=kv_send,
-            recv_sem=kv_recv.at[direction, step - 1],
+            send_sem=kv_send.at[direction, part, step - 1],
+            recv_sem=kv_recv.at[direction, part, step - 1],
             device_id={"sp": right if direction == 0 else left},
             device_id_type=MESH,
         )
@@ -156,8 +174,20 @@
         start = block_at(direction, back) * w_rows + half * half_rows
         return pl.ds(pl.multiple_of(start, half_rows), half_rows)
 
-    def w_copy(ref, send, recv, direction, step, back, half):
-        part = ref.at[half_of(direction, back, half)]
+    quarter = half_rows // 2
+    groups = first_steps // 4
+    early = 3 * groups
+    shared = max(0, early - BEHIND)
+
+    def d_part(direction, back, part):
+        if part == 0:
+            return half_of(direction, back, 0)
+        which = parity if part == 1 else 1 - parity
+        start = block_at(direction, back) * w_rows + half_rows + which * quarter
+        return pl.ds(pl.multiple_of(start, quarter), quarter)
+
+    def w_copy(ref, send, recv, direction, step, half, rows_of):
+        part = ref.at[rows_of]
         return pltpu.make_async_remote_copy(
             src_ref=part,
             dst_ref=part,
@@ -167,6 +197,12 @@
             device_id_type=MESH,
         )
 
+    def m_copy(direction, step, back, half):
+        return w_copy(m_all, m_send, m_recv, direction, step, half, half_of(direction, back, half))
+
+    def d_copy(direction, step, back, half):
+        return w_copy(d_all, d_send, d_recv, direction, step, half, d_part(direction, back, half))
+
     def steps_of(direction, flipped):
         return first_steps if direction == int(flipped) else second_steps
 
@@ -177,53 +213,101 @@
         else:
             pl.when(condition)(body)
 
+    def both(a, b):
+        return (a and b) if isinstance(a, bool) else a & b
+
+    def kv_moves(direction, step, back):
+        if direction == 0:
+            return (i >= back) & (i < n - 1) & (step <= first_steps)
+        return (lax.rem(i + back, n) < second_steps) & (step <= second_steps)
+
     def kv_slot(s):
+        for part in (0, 1):
+
+            @pl.when((i >= s) & (s <= first_steps))
+            def _(part=part):
+                kv_copy(0, s, s, part).wait_recv()
+
+            @pl.when(kv_moves(0, s + 1, s))
+            def _(part=part):
+                kv_copy(0, s + 1, s, part).start()
+
+            @pl.when((lax.rem(i + s, n) < second_steps) & (s <= second_steps))
+            def _(part=part):
+                kv_copy(1, s, s, part).wait_recv()
+
+            @pl.when(kv_moves(1, s + 1, s))
+            def _(part=part):
+                kv_copy(1, s + 1, s, part).start()
+
         for direction in (0, 1):
-            count = steps_of(direction, False)
-
-            def arrived(direction=direction, count=count):
-                kv_copy(direction, s, s).wait_recv()
-                if_step(s < count, lambda: kv_copy(direction, s + 1, s).start())
-
-            if_step(s <= count, arrived)
-
-    def w_arrived(ref, send, recv, s, half, direction, count):
-        w_copy(ref, send, recv, direction, s, s, half).wait_recv()
-        if_step(s < count, lambda: w_copy(ref, send, recv, direction, s + 1, s, half).start())
-
-    def to_partner(s, half, direction):
-        part = m_all.at[half_of(direction, s, half)]
+
+            @pl.when(kv_moves(direction, s, s - 1))
+            def _(direction=direction):
+                for part in (0, 1):
+                    kv_copy(direction, s, s - 1, part).wait_send()
+
+    def w_arrived(copy, s, half, direction, count):
+        copy(direction, s, s, half).wait_recv()
+        if_step(s < count, lambda: copy(direction, s + 1, s, half).start())
+
+    def to_partner(src, dst, rows_of, send, recv, s):
         pltpu.make_async_remote_copy(
-            src_ref=part,
-            dst_ref=o_all.at[half_of(direction, s, half)],
-            send_sem=y_send,
-            recv_sem=y_recv.at[s - 1],
+            src_ref=src.at[rows_of],
+            dst_ref=dst.at[rows_of],
+            send_sem=send,
+            recv_sem=recv.at[s - 1],
             device_id={"grp": partner},
             device_id_type=MESH,
         ).start()
 
+    def wait_down(start, stop):
+        for d in range(start, stop):
+            blocks = int(d <= first_steps) + int(d <= second_steps)
+            rest = d_all.at[pl.ds(0, blocks * quarter)]
+            pltpu.make_async_copy(rest, rest, dy_recv.at[d - 1]).wait()
+
     def w_slot(s, half):
         for direction in (0, 1):
 
             def m_arrived(direction=direction, count=steps_of(direction, True)):
-                w_arrived(m_all, m_send, m_recv, s, half, direction, count)
-                to_partner(s, half, direction)
+                w_arrived(m_copy, s, half, direction, count)
+                to_partner(m_all, o_all, half_of(direction, s, half), y_send, y_recv, s)
 
             if_step(s <= steps_of(direction, True), m_arrived)
+        d = s - BEHIND
+        if half == 0 and isinstance(d, int) and d == shared + 1 and shared > 0:
+            wait_down(shared, shared + 1)
+            for direction in (0, 1):
+                if d <= steps_of(direction, False):
+                    d_copy(direction, d, shared, 2).start()
+        for part in (1,) if half == 0 else (0, 2):
+            for direction in (0, 1):
+
+                def d_arrived(direction=direction, part=part, count=steps_of(direction, False)):
+                    w_arrived(d_copy, d, part, direction, count)
+                    if part == 1 and (not isinstance(d, int) or d <= shared):
+                        to_partner(d_all, d_all, d_part(direction, d, 1), dy_send, dy_recv, d)
+
+                if part == 2 and not isinstance(d, int):
+                    continue
+                if part == 2 and d <= shared:
+                    continue
+                if_step(both(d > 0, d <= steps_of(direction, False)), d_arrived)
+
+        def d_first():
+            for part in (1,) if half == 0 else (0, 2) if shared == 0 else (0,):
+                for direction in (0, 1):
+                    d_copy(direction, 1, 0, part).start()
+
+        if_step(s == BEHIND, d_first)
+
+    for part in (0, 1):
         for direction in (0, 1):
-
-            def d_arrived(direction=direction, count=steps_of(direction, False)):
-                w_arrived(d_all, d_send, d_recv, s, half, direction, count)
-
-            if_step(s <= steps_of(direction, False), d_arrived)
-
-    for direction in (0, 1):
-        kv_copy(direction, 1, 0).start()
+            pl.when(kv_moves(direction, 1, 0))(kv_copy(direction, 1, 0, part).start)
     for half in (0, 1):
         for direction in (0, 1):
-            w_copy(m_all, m_send, m_recv, direction, 1, 0, half).start()
-        for direction in (0, 1):
-            w_copy(d_all, d_send, d_recv, direction, 1, 0, half).start()
+            m_copy(direction, 1, 0, half).start()
 
     def ow_block(index):
         return ow_all.at[pl.ds(pl.multiple_of(index * width, width), width)]
@@ -241,6 +325,12 @@
     for k in range(2, t, 2):
         ow_copy(c, peer(k), ow_send, ow_recv).start()
     ow_copy(c, sibling, ow_pass_send, ow_pass_recv).start()
+
+    def ow_pass():
+        x_rows = ow_all.at[pl.ds(0, (t // 2 - 1) * width)]
+        pltpu.make_async_copy(x_rows, x_rows, ow_recv).wait()
+        for k in range(2, t, 2):
+            ow_copy(peer(k), sibling, ow_pass_send, ow_pass_recv).start()
 
     scale = width ** (-0.5)
 
@@ -291,6 +381,8 @@
 
     def group(g, carry):
         s, w = 4 * g, 3 * g
+        if t > 2:
+            pl.when(g == groups - 1)(ow_pass)
         with jax.named_scope("kv1"):
             kv_slot(s + 1)
         attend_near(s + 1)
@@ -321,8 +413,6 @@
         attend_far(s + 4)
         return carry
 
-    groups = first_steps // 4
-    early = 3 * groups
     lax.fori_loop(0, groups, group, 0)
 
     def columns(index, size):
@@ -331,11 +421,6 @@
     def send_attended():
         own = columns(c, width)
         att_all[:, own] = (acc_near[...] + jnp.exp(run_near[...]) * acc_far[...]).astype(BF16)
-        if t > 2:
-            x_rows = ow_all.at[pl.ds(0, (t // 2 - 1) * width)]
-            pltpu.make_async_copy(x_rows, x_rows, ow_recv).wait()
-            for k in range(2, t, 2):
-                ow_copy(peer(k), sibling, ow_pass_send, ow_pass_recv).start()
         for k in range(1, t):
             pltpu.make_async_remote_copy(
                 src_ref=att_all.at[:, own],
@@ -410,10 +495,89 @@
 
         lax.fori_loop(0, tok // chunk, step, 0)
 
-    count = d_model // wide
-    own = pl.ds(pl.multiple_of(c * own_rows, own_rows), own_rows)
-
-    def partial(p, carry):
+    count, chips = d_model // wide, t // 2
+    half_of_rows = tok // 2
+    core, chip = lax.rem(c, 2), c // 2
+
+    def rows_at(start, size):
+        return pl.ds(pl.multiple_of(start, own_rows), size)
+
+    own_half = rows_at(core * half_of_rows, half_of_rows)
+    other_half = rows_at((1 - core) * half_of_rows, half_of_rows)
+    in_half = rows_at(chip * own_rows, own_rows)
+    own = rows_at(core * half_of_rows + chip * own_rows, own_rows)
+
+    def to_peer(src, dst, send, recv, where):
+        pltpu.make_async_remote_copy(
+            src_ref=src,
+            dst_ref=dst,
+            send_sem=send,
+            recv_sem=recv,
+            device_id={"tp": where},
+            device_id_type=MESH,
+        ).start()
+
+    def await_all(ref, sem):
+        pltpu.make_async_copy(ref, ref, sem).wait()
+
+    whole_at = first_steps - BEHIND
+    first_tiles = max(0, min(count, (2 * whole_at + 2 - per_chunk) // per_chunk))
+    first_tile = (i + n - whole_at + per_chunk - 1) // per_chunk
+
+    def partial(j, carry):
+        p = lax.rem(first_tile + j, count)
+        parts[p] = lax.dot_general(
+            hidden[...],
+            d_all[columns(p, wide), :],
+            (((1,), (1,)), ((), ())),
+            preferred_element_type=F32,
+        ).astype(BF16)
+        to_peer(parts.at[p, other_half], core_buf.at[p], cs_send, cs_recv.at[p], sibling)
+        return carry
+
+    def between_cores(j, carry):
+        p = lax.rem(first_tile + j, count)
+        await_all(core_buf.at[p], cs_recv.at[p])
+        halves[p] = (parts[p, own_half, :].astype(F32) + core_buf[p].astype(F32)).astype(BF16)
+        for far in range(1, chips):
+            to = lax.rem(chip + far, chips)
+            to_peer(
+                halves.at[p, rows_at(to * own_rows, own_rows)],
+                rs_buf.at[p, far - 1],
+                rs_send,
+                rs_recv.at[p],
+                2 * to + core,
+            )
+        return carry
+
+    def between_chips(j, carry):
+        p = lax.rem(first_tile + j, count)
+        total = halves[p, in_half, :].astype(F32)
+        if chips > 1:
+            await_all(rs_buf.at[p], rs_recv.at[p])
+        for far in range(1, chips):
+            total = total + rs_buf[p, far - 1].astype(F32)
+        ffn[p, own, :] = total.astype(BF16)
+        return p
+
+    def chips_then_cores(j, carry):
+        p = between_chips(j, carry)
+        for far in range(1, chips):
+            to = 2 * lax.rem(chip + far, chips) + core
+            to_peer(ffn.at[p, own], ffn.at[p, own], ag_send, ag_recv.at[p], to)
+        return carry
+
+    def to_all(p):
+        for far in range(1, t):
+            to_peer(ffn.at[p, own], ffn.at[p, own], lg_send.at[p], lg_recv.at[p], peer(far))
+
+    def chips_then_all(j, carry):
+        to_all(between_chips(j, carry))
+        return carry
+
+    def last_partial(j):
+        p = lax.rem(first_tile + j, count)
+        k = j - (count - LAST)
         parts[p] = lax.dot_general(
             hidden[...],
             d_all[columns(p, wide), :],
@@ -421,32 +585,31 @@
             preferred_element_type=F32,
         ).astype(BF16)
         for far in range(1, t):
-            rows_of = pl.ds(pl.multiple_of(peer(far) * own_rows, own_rows), own_rows)
-            pltpu.make_async_remote_copy(
-                src_ref=parts.at[p, rows_of],
-                dst_ref=rs_buf.at[p, far - 1],
-                send_sem=rs_send,
-                recv_sem=rs_recv.at[p],
-                device_id={"tp": peer(far)},
-                device_id_type=MESH,
-            ).start()
-        return carry
-
-    def total_of(p, carry):
-        pltpu.make_async_copy(rs_buf.at[p], rs_buf.at[p], rs_recv.at[p]).wait()
+            to = peer(far)
+            start = lax.rem(to, 2) * half_of_rows + to // 2 * own_rows
+            to_peer(
+                parts.at[p, rows_at(start, own_rows)],
+                rs_last.at[k, far - 1],
+                ls_send,
+                ls_recv.at[k],
+                to,
+            )
+
+    def last_total(j):
+        p = lax.rem(first_tile + j, count)
+        k = j - (count - LAST)
+        await_all(rs_last.at[k], ls_recv.at[k])
         total = parts[p, own, :].astype(F32)
         for far in range(1, t):
-            total = total + rs_buf[p, far - 1].astype(F32)
+            total = total + rs_last[k, far - 1].astype(F32)
         ffn[p, own, :] = total.astype(BF16)
-        for far in range(1, t):
-            pltpu.make_async_remote_copy(
-                src_ref=ffn.at[p, own],
-                dst_ref=ffn.at[p, own],
-                send_sem=ag_send,
-                recv_sem=ag_recv.at[p],
-                device_id={"tp": peer(far)},
-                device_id_type=MESH,
-            ).start()
+        to_all(p)
+
+    def to_other_core(j, carry):
+        p = lax.rem(first_tile + j, count)
+        if chips > 1:
+            await_all(rs_buf.at[p], ag_recv.at[p])
+        to_peer(ffn.at[p, own_half], ffn.at[p, own_half], cg_send, cg_recv.at[p], sibling)
         return carry
 
     def zero_acts():
@@ -478,39 +641,81 @@
             lambda: act_of(o_all, o_act, 0, arrived_chunks),
         ),
     ]
+    after = [
+        named("mine3", lambda: act_of(m_all, m_act, arrived_chunks, chunks)),
+        named(
+            "other2",
+            lambda: wait_other(early + 1, first_steps + 1),
+            lambda: act_of(o_all, o_act, arrived_chunks, chunks),
+            hide,
+            lambda: wait_down(1, shared),
+        ),
+    ]
+    stages = {"partial": partial, "cores": between_cores}
+    reached = dict.fromkeys(stages, 0)
+    reduced = count - LAST
+    near = min(first_tiles, reduced)
+    third = (near + 2) // 3
+    two = min(2 * third, near)
+
+    def up_to(name, stop):
+        def body():
+            if reached[name] < stop:
+                lax.fori_loop(reached[name], stop, stages[name], 0)
+                reached[name] = stop
+
+        return named(name, body)
+
+    after += [
+        up_to("partial", third),
+        up_to("partial", two),
+        lambda: (up_to("partial", near)(), up_to("cores", third)()),
+        up_to("cores", two),
+    ]
     with jax.named_scope("send_attended"):
         send_attended()
-    for s in range(early + 1, first_steps + 1):
+    for s in range(early + 1, first_steps + BEHIND + 1):
         for half in (0, 1):
-            with jax.named_scope("wl"):
+            with jax.named_scope("wl" if s <= first_steps else "dl"):
                 w_slot(s, half)
-            if tasks:
+            if s == first_steps and half == 1:
+                while tasks:
+                    tasks.pop(0)()
+                tasks = after
+            elif tasks:
                 tasks.pop(0)()
     while tasks:
         tasks.pop(0)()
-    with jax.named_scope("mine3"):
-        act_of(m_all, m_act, arrived_chunks, chunks)
-    with jax.named_scope("other2"):
-        wait_other(early + 1, first_steps + 1)
-        act_of(o_all, o_act, arrived_chunks, chunks)
-    with jax.named_scope("hide"):
-        hide()
-    with jax.named_scope("partial"):
-        lax.fori_loop(0, count, partial, 0)
-    with jax.named_scope("total"):
-        lax.fori_loop(0, count, total_of, 0)
+    up_to("partial", reduced)()
+    with jax.named_scope("last_partial"):
+        for j in range(reduced, count):
+            last_partial(j)
+    up_to("cores", reduced)()
+    with jax.named_scope("chips"):
+        lax.fori_loop(0, two, chips_then_cores, 0)
+    with jax.named_scope("last_total"):
+        for j in range(reduced, count):
+            last_total(j)
+    with jax.named_scope("chips_all"):
+        lax.fori_loop(two, reduced, chips_then_all, 0)
+    with jax.named_scope("back"):
+        lax.fori_loop(0, two, to_other_core, 0)
 
     with jax.named_scope("gathered"):
-        for p in range(count):
-            others = rs_buf.at[p]
-            pltpu.make_async_copy(others, others, ag_recv.at[p]).wait()
+        for j in range(count):
+            p = lax.rem(first_tile + j, count)
+            if j < two:
+                await_all(core_buf.at[p], cg_recv.at[p])
+            else:
+                await_all(rs_last.at[0], lg_recv.at[p])
 
     def finish(j, carry):
         at = columns(j, chunk)
         x = jnp.concatenate([ffn[p, at, :] for p in range(count)], axis=1).astype(F32)
-        out_ref[at, :] = (
+        out[at, :] = (
             middle[at, :].astype(F32) + out_gain_ref[...] * normalize(x)
         ).astype(BF16)
+        pltpu.make_async_copy(out.at[at], out_ref.at[at], out_sem).start()
         return carry
 
     with jax.named_scope("finish"):
@@ -519,17 +724,30 @@
     def drain(ref, sem):
         pltpu.make_async_copy(ref, ref, sem).wait()
 
-    drain(kv_all.at[pl.ds(0, n - 1)], kv_send)
     ring = pl.ds(0, (n - 1) * w_rows)
     drain(m_all.at[ring], m_send)
     drain(m_all.at[ring], y_send)
-    drain(d_all.at[ring], d_send)
+    over_y = min(shared, first_steps) + min(shared, second_steps)
+    d_rows = (n - 1) * w_rows - over_y * quarter
+    drain(d_all.at[pl.ds(0, d_rows)], d_send)
+    if over_y:
+        drain(d_all.at[pl.ds(0, over_y * quarter)], dy_send)
     if t > 2:
         drain(ow_all.at[pl.ds(0, (t // 2 - 1) * width)], ow_send)
     drain(ow_all.at[pl.ds(0, (t // 2) * width)], ow_pass_send)
     drain(att_all.at[:, pl.ds(0, (t - 1) * width)], att_send)
-    drain(rs_buf, rs_send)
-    drain(rs_buf, ag_send)
+    if reduced:
+        drain(core_buf.at[pl.ds(0, reduced)], cs_send)
+        if chips > 1:
+            drain(rs_buf.at[pl.ds(0, reduced)], rs_send)
+    if two:
+        drain(core_buf.at[pl.ds(0, two)], cg_send)
+        if chips > 1:
+            drain(rs_buf.at[pl.ds(0, two)], ag_send)
+    drain(rs_last, ls_send)
+    for j in range(two, count):
+        drain(rs_last.at[0], lg_send.at[lax.rem(first_tile + j, count)])
+    pltpu.make_async_copy(out, out_ref, out_sem).wait()
 
 
 def solution(mesh):
@@ -555,7 +773,6 @@
         tile = 128
         count = d_model // WIDE
         logit = jnp.broadcast_to(key_logit.reshape(1, tok), (16, tok))
-        vmem = pl.BlockSpec(memory_space=pltpu.VMEM)
         hbm = pl.BlockSpec(memory_space=pltpu.HBM)
         steps = n // 2
         dma = pltpu.SemaphoreType.DMA
@@ -563,7 +780,7 @@
             functools.partial(layer_kernel, (n, t)),
             out_shape=jax.ShapeDtypeStruct((tok, d_model), BF16),
             in_specs=[hbm] * 12,
-            out_specs=vmem,
+            out_specs=hbm,
             scratch_shapes=[
                 pltpu.VMEM((tok, width), BF16),
                 pltpu.VMEM((tok, d_model), BF16),
@@ -583,20 +800,22 @@
                 pltpu.VMEM((tok, units), F32),
                 pltpu.VMEM((tok, units), BF16),
                 pltpu.VMEM((count, tok, WIDE), BF16),
-                pltpu.VMEM((count, t - 1, tok // t, WIDE), BF16),
+                pltpu.VMEM((count, tok // 2, WIDE), BF16),
+                pltpu.VMEM((count, tok // 2, WIDE), BF16),
+                pltpu.VMEM((count, max(t // 2 - 1, 1), tok // t, WIDE), BF16),
                 pltpu.VMEM((count, tok, WIDE), BF16),
                 pltpu.VMEM((tile, 2 * tile), BF16),
                 pltpu.VMEM((tok, width), F32),
                 pltpu.VMEM((tok, width), F32),
                 pltpu.VMEM((tok, width), F32),
                 dma((12,)),
-                dma,
-                dma((2, steps)),
-                dma,
                 dma((2, 2, steps)),
-                dma,
                 dma((2, 2, steps)),
                 dma,
+                dma((2, 2, steps)),
+                dma,
+                dma((2, 3, steps)),
+                dma,
                 dma((steps,)),
                 dma,
                 dma,
@@ -607,6 +826,19 @@
                 dma,
                 dma((count,)),
                 dma,
+                dma((count,)),
+                dma,
+                dma((count,)),
+                dma,
+                dma((count,)),
+                dma,
+                dma((steps,)),
+                pltpu.VMEM((tok, d_model), BF16),
+                dma,
+                pltpu.VMEM((LAST, t - 1, tok // t, WIDE), BF16),
+                dma,
+                dma((LAST,)),
+                dma((count,)),
                 dma((count,)),
             ],
             compiler_params=pltpu.CompilerParams(

time: 157 us -> 153 us (0.975)
  Pallas kernels: 154 us -> 150 us
    pallas_call x1, Pallas kernels: 154 us -> 150 us  [shards(): pl.pallas_call(functools.partial(layer_kernel, (n, t)), out_shape=jax.Sha...]
where the time goes in v3:
time: 153 us
  Pallas kernels  150 us (98%)
  local copies, waits for them, and re-layouts  3.13 us (2%)
    pallas_call x1, Pallas kernels, shards(): pl.pallas_call(functools.partial(layer_kernel, (n, t)), out_shape=jax.Sha...  150 us

profile of v3, /device:TPU:33, one launch (start us, length us, event | category | flops | bytes accessed | tf_op | source)
XLA Modules:
  0.0 153.1 jit_solution(8129040044278782486)
XLA Ops:
  0.0 0.0 copy-start
  0.0 0.7 copy-done
  0.7 0.6 broadcast_in_dim.8.lg_ref
  1.3 149.9 %layer.1 = bf16[128,2048]{1,0:T(8,128)(2,1)} custom-call(bf16[128,128]{1,0:T(8,128)(2,1)} %q_in.1, bf16[128,128]{1,0:T(8,128)(2,1)} %k_ref.1, bf16[128,128]{1,0:T(8,128)(2,1)} %v_ref.1, bf16[16,128]{1,0:T(8,128)(2,1)} %broadcast_in_dim.8.lg_ref, bf16[128,2048]{1,0:T(8,128)(2,1)} %res_in.1, bf16[128,2048]{1,0:T(8,128)(2,1)} %ow_ref.1, f32[1,2048]{1,0:T(1,128)} %bitcast.4, ...), custom_call_target="tpu_custom_call" | custom-call | tf_op jit(solution)/shard_map/layer/pallas_call | solution.py:779
  151.2 1.9 %copy.14 = bf16[128,2048]{1,0:T(8,128)(2,1)} copy(bf16[128,2048]{1,0:T(8,128)(2,1)} %layer.1) | data formatting | bytes 1048576
Async XLA Ops:
  0.0 0.7 copy-start

commit v4 on v3

--- a/solution.py
+++ b/solution.py
@@ -12,8 +12,10 @@
 F32 = jnp.float32
 BF16 = jnp.bfloat16
 WIDE = 256
+LOGIT_ROWS = 8
+CHUNK = 32
 LAST = 2
-BEHIND = 3
+BEHIND = 2
 
 
 def layer_kernel(
@@ -112,7 +114,7 @@
     copies = [
         pltpu.make_async_copy(k_ref, kv_own.at[pl.ds(0, tok)], local_sem.at[0]),
         pltpu.make_async_copy(v_ref, kv_own.at[pl.ds(tok, tok)], local_sem.at[1]),
-        pltpu.make_async_copy(lg_ref, kv_own.at[pl.ds(2 * tok, 16)], local_sem.at[2]),
+        pltpu.make_async_copy(lg_ref, kv_own.at[pl.ds(2 * tok, LOGIT_ROWS)], local_sem.at[2]),
         pltpu.make_async_copy(down_ref, d_all.at[w_own], local_sem.at[3]),
         pltpu.make_async_copy(
             ow_ref, ow_all.at[pl.ds(pl.multiple_of(c * width, width), width)], local_sem.at[4]
@@ -158,14 +160,17 @@
     def block_at(direction, back):
         return lax.rem(i + n - back, n) if direction == 0 else lax.rem(i + back, n)
 
+    def turn(step, turns):
+        return (step - 1) % turns if isinstance(step, int) else lax.rem(step - 1, turns)
+
     def kv_copy(direction, step, back, part):
-        rows_of = pl.ds(0, tok) if part == 0 else pl.ds(tok, tok + 16)
+        rows_of = pl.ds(0, tok) if part == 0 else pl.ds(tok, tok + LOGIT_ROWS)
         block = kv_all.at[block_at(direction, back), rows_of]
         return pltpu.make_async_remote_copy(
             src_ref=block,
             dst_ref=block,
-            send_sem=kv_send.at[direction, part, step - 1],
-            recv_sem=kv_recv.at[direction, part, step - 1],
+            send_sem=kv_send.at[direction, part, turn(step, 2)],
+            recv_sem=kv_recv.at[direction, part, turn(step, 8)],
             device_id={"sp": right if direction == 0 else left},
             device_id_type=MESH,
         )
@@ -192,7 +197,7 @@
             src_ref=part,
             dst_ref=part,
             send_sem=send,
-            recv_sem=recv.at[direction, half, step - 1],
+            recv_sem=recv.at[direction, half, turn(step, 4)],
             device_id={"sp": right if direction == 0 else left},
             device_id_type=MESH,
         )
@@ -251,49 +256,58 @@
         copy(direction, s, s, half).wait_recv()
         if_step(s < count, lambda: copy(direction, s + 1, s, half).start())
 
-    def to_partner(src, dst, rows_of, send, recv, s):
+    def to_partner(src, dst, rows_of, send, recv):
         pltpu.make_async_remote_copy(
             src_ref=src.at[rows_of],
             dst_ref=dst.at[rows_of],
             send_sem=send,
-            recv_sem=recv.at[s - 1],
+            recv_sem=recv,
             device_id={"grp": partner},
             device_id_type=MESH,
         ).start()
 
-    def wait_down(start, stop):
-        for d in range(start, stop):
-            blocks = int(d <= first_steps) + int(d <= second_steps)
+    def wait_down(start, stop, which):
+        blocks = min(stop - 1, first_steps) + min(stop - 1, second_steps)
+        blocks -= min(start - 1, first_steps) + min(start - 1, second_steps)
+        if blocks > 0:
             rest = d_all.at[pl.ds(0, blocks * quarter)]
-            pltpu.make_async_copy(rest, rest, dy_recv.at[d - 1]).wait()
+            pltpu.make_async_copy(rest, rest, dy_recv.at[which]).wait()
 
     def w_slot(s, half):
-        for direction in (0, 1):
-
-            def m_arrived(direction=direction, count=steps_of(direction, True)):
-                w_arrived(m_copy, s, half, direction, count)
-                to_partner(m_all, o_all, half_of(direction, s, half), y_send, y_recv, s)
-
-            if_step(s <= steps_of(direction, True), m_arrived)
         d = s - BEHIND
-        if half == 0 and isinstance(d, int) and d == shared + 1 and shared > 0:
-            wait_down(shared, shared + 1)
+
+        def m_parts():
             for direction in (0, 1):
-                if d <= steps_of(direction, False):
-                    d_copy(direction, d, shared, 2).start()
-        for part in (1,) if half == 0 else (0, 2):
-            for direction in (0, 1):
-
-                def d_arrived(direction=direction, part=part, count=steps_of(direction, False)):
-                    w_arrived(d_copy, d, part, direction, count)
-                    if part == 1 and (not isinstance(d, int) or d <= shared):
-                        to_partner(d_all, d_all, d_part(direction, d, 1), dy_send, dy_recv, d)
-
-                if part == 2 and not isinstance(d, int):
-                    continue
-                if part == 2 and d <= shared:
-                    continue
-                if_step(both(d > 0, d <= steps_of(direction, False)), d_arrived)
+
+                def m_arrived(direction=direction, count=steps_of(direction, True)):
+                    w_arrived(m_copy, s, half, direction, count)
+                    y_sem = y_recv.at[0 if not isinstance(s, int) or s <= early else 1]
+                    to_partner(m_all, o_all, half_of(direction, s, half), y_send, y_sem)
+
+                if_step(s <= steps_of(direction, True), m_arrived)
+        def d_parts():
+            if half == 0 and isinstance(d, int) and d == shared + 1 and shared > 0:
+                wait_down(shared, shared + 1, 1)
+                for direction in (0, 1):
+                    if d <= steps_of(direction, False):
+                        d_copy(direction, d, shared, 2).start()
+            for part in (1,) if half == 0 else (0, 2):
+                for direction in (0, 1):
+
+                    def d_arrived(direction=direction, part=part, count=steps_of(direction, False)):
+                        w_arrived(d_copy, d, part, direction, count)
+                        if part == 1 and (not isinstance(d, int) or d <= shared):
+                            dy_sem = dy_recv.at[int(d == shared) if isinstance(d, int) else (d == shared).astype(jnp.int32)]
+                            to_partner(d_all, d_all, d_part(direction, d, 1), dy_send, dy_sem)
+
+                    if part == 2 and not isinstance(d, int):
+                        continue
+                    if part == 2 and d <= shared:
+                        continue
+                    if_step(both(d > 0, d <= steps_of(direction, False)), d_arrived)
+
+        for body in (d_parts, m_parts) if half == 0 else (m_parts, d_parts):
+            body()
 
         def d_first():
             for part in (1,) if half == 0 else (0, 2) if shared == 0 else (0,):
@@ -337,7 +351,7 @@
     def terms(block, causal):
         k = kv_all[block, pl.ds(0, tok), :]
         v = kv_all[block, pl.ds(tok, tok), :]
-        logit = kv_all[block, pl.ds(2 * tok, 16), :].astype(F32)[0:1, :]
+        logit = kv_all[block, pl.ds(2 * tok, LOGIT_ROWS), :].astype(F32)[0:1, :]
         scores = lax.dot_general(
             q_ref[...], k, (((1,), (1,)), ((), ())), preferred_element_type=F32
         )
@@ -451,7 +465,7 @@
     def normalize(x):
         return x * lax.rsqrt(jnp.mean(x * x, axis=-1, keepdims=True) + EPSILON)
 
-    chunk = 16
+    chunk = CHUNK
 
     def norms(start, stop):
         def step(j, carry):
@@ -478,11 +492,12 @@
 
         lax.fori_loop(start, stop, step, 0)
 
-    def wait_other(start, stop):
-        for s in range(start, stop):
-            blocks = int(s <= first_steps) + int(s <= second_steps)
+    def wait_other(start, stop, which):
+        blocks = min(stop - 1, first_steps) + min(stop - 1, second_steps)
+        blocks -= min(start - 1, first_steps) + min(start - 1, second_steps)
+        if blocks:
             rest = o_all.at[pl.ds(0, blocks * w_rows)]
-            pltpu.make_async_copy(rest, rest, y_recv.at[s - 1]).wait()
+            pltpu.make_async_copy(rest, rest, y_recv.at[which]).wait()
 
     def hide():
         def step(j, carry):
@@ -637,7 +652,7 @@
         named("mine2", lambda: act_of(m_all, m_act, some, arrived_chunks)),
         named(
             "other1",
-            lambda: wait_other(1, early + 1),
+            lambda: wait_other(1, early + 1, 0),
             lambda: act_of(o_all, o_act, 0, arrived_chunks),
         ),
     ]
@@ -645,10 +660,10 @@
         named("mine3", lambda: act_of(m_all, m_act, arrived_chunks, chunks)),
         named(
             "other2",
-            lambda: wait_other(early + 1, first_steps + 1),
+            lambda: wait_other(early + 1, first_steps + 1, 1),
             lambda: act_of(o_all, o_act, arrived_chunks, chunks),
             hide,
-            lambda: wait_down(1, shared),
+            lambda: wait_down(1, shared, 0),
         ),
     ]
     stages = {"partial": partial, "cores": between_cores}
@@ -772,9 +787,8 @@
         d_model = residual.shape[1]
         tile = 128
         count = d_model // WIDE
-        logit = jnp.broadcast_to(key_logit.reshape(1, tok), (16, tok))
+        logit = jnp.broadcast_to(key_logit.reshape(1, tok), (LOGIT_ROWS, tok))
         hbm = pl.BlockSpec(memory_space=pltpu.HBM)
-        steps = n // 2
         dma = pltpu.SemaphoreType.DMA
         return pl.pallas_call(
             functools.partial(layer_kernel, (n, t)),
@@ -787,7 +801,7 @@
                 pltpu.VMEM((1, d_model), F32),
                 pltpu.VMEM((1, d_model), F32),
                 pltpu.VMEM((1, d_model), F32),
-                pltpu.VMEM((n, 2 * tok + 16, width), BF16),
+                pltpu.VMEM((n, 2 * tok + LOGIT_ROWS, width), BF16),
                 pltpu.VMEM((n * w_rows, units), BF16),
                 pltpu.VMEM((n * w_rows, units), BF16),
                 pltpu.VMEM((n * w_rows, units), BF16),
@@ -809,14 +823,14 @@
                 pltpu.VMEM((tok, width), F32),
                 pltpu.VMEM((tok, width), F32),
                 dma((12,)),
-                dma((2, 2, steps)),
-                dma((2, 2, steps)),
-                dma,
-                dma((2, 2, steps)),
-                dma,
-                dma((2, 3, steps)),
-                dma,
-                dma((steps,)),
+                dma((2, 2, 2)),
+                dma((2, 2, 8)),
+                dma,
+                dma((2, 2, 4)),
+                dma,
+                dma((2, 3, 4)),
+                dma,
+                dma((2,)),
                 dma,
                 dma,
                 dma,
@@ -832,7 +846,7 @@
                 dma,
                 dma((count,)),
                 dma,
-                dma((steps,)),
+                dma((2,)),
                 pltpu.VMEM((tok, d_model), BF16),
                 dma,
                 pltpu.VMEM((LAST, t - 1, tok // t, WIDE), BF16),

time: 153 us -> 149 us (0.974)
  Pallas kernels: 150 us -> 146 us
    pallas_call x1, Pallas kernels: 150 us -> 146 us  [shards(): pl.pallas_call(functools.partial(layer_kernel, (n, t)), out_shape=jax.Sha...]
where the time goes in v4:
time: 149 us
  Pallas kernels  146 us (98%)
  local copies, waits for them, and re-layouts  3.12 us (2%)
    pallas_call x1, Pallas kernels, shards(): pl.pallas_call(functools.partial(layer_kernel, (n, t)), out_shape=jax.Sha...  146 us

profile of v4, /device:TPU:33, one launch (start us, length us, event | category | flops | bytes accessed | tf_op | source)
XLA Modules:
  0.0 148.7 jit_solution(8435571417965795912)
XLA Ops:
  0.0 0.0 copy-start
  0.0 0.7 copy-done
  0.7 0.6 broadcast_in_dim.8.lg_ref
  1.2 145.6 %layer.1 = bf16[128,2048]{1,0:T(8,128)(2,1)} custom-call(bf16[128,128]{1,0:T(8,128)(2,1)} %q_in.1, bf16[128,128]{1,0:T(8,128)(2,1)} %k_ref.1, bf16[128,128]{1,0:T(8,128)(2,1)} %v_ref.1, bf16[8,128]{1,0:T(8,128)(2,1)} %broadcast_in_dim.8.lg_ref, bf16[128,2048]{1,0:T(8,128)(2,1)} %res_in.1, bf16[128,2048]{1,0:T(8,128)(2,1)} %ow_ref.1, f32[1,2048]{1,0:T(1,128)} %bitcast.4, ...), custom_call_target="tpu_custom_call" | custom-call | tf_op jit(solution)/shard_map/layer/pallas_call | solution.py:793
  146.8 1.9 %copy.14 = bf16[128,2048]{1,0:T(8,128)(2,1)} copy(bf16[128,2048]{1,0:T(8,128)(2,1)} %layer.1) | data formatting | bytes 1048576
Async XLA Ops:
  0.0 0.7 copy-start

commit v5 on v4

--- a/solution.py
+++ b/solution.py
@@ -15,7 +15,7 @@
 LOGIT_ROWS = 8
 CHUNK = 32
 LAST = 2
-BEHIND = 2
+BEHIND = 1
 
 
 def layer_kernel(
@@ -273,6 +273,11 @@
             rest = d_all.at[pl.ds(0, blocks * quarter)]
             pltpu.make_async_copy(rest, rest, dy_recv.at[which]).wait()
 
+    def d_first(half):
+        for part in (1,) if half == 0 else (0, 2) if shared == 0 else (0,):
+            for direction in (0, 1):
+                d_copy(direction, 1, 0, part).start()
+
     def w_slot(s, half):
         d = s - BEHIND
 
@@ -309,12 +314,7 @@
         for body in (d_parts, m_parts) if half == 0 else (m_parts, d_parts):
             body()
 
-        def d_first():
-            for part in (1,) if half == 0 else (0, 2) if shared == 0 else (0,):
-                for direction in (0, 1):
-                    d_copy(direction, 1, 0, part).start()
-
-        if_step(s == BEHIND, d_first)
+        if_step(s == BEHIND, lambda: d_first(half))
 
     for part in (0, 1):
         for direction in (0, 1):
@@ -322,6 +322,8 @@
     for half in (0, 1):
         for direction in (0, 1):
             m_copy(direction, 1, 0, half).start()
+        if BEHIND == 0:
+            d_first(half)
 
     def ow_block(index):
         return ow_all.at[pl.ds(pl.multiple_of(index * width, width), width)]

time: 149 us -> 147 us (0.987)
  Pallas kernels: 146 us -> 144 us
    pallas_call x1, Pallas kernels: 146 us -> 144 us  [shards(): pl.pallas_call(functools.partial(layer_kernel, (n, t)), out_shape=jax.Sha...]
where the time goes in v5:
time: 147 us
  Pallas kernels  144 us (98%)
  local copies, waits for them, and re-layouts  3.12 us (2%)
    pallas_call x1, Pallas kernels, shards(): pl.pallas_call(functools.partial(layer_kernel, (n, t)), out_shape=jax.Sha...  144 us

profile of v5, /device:TPU:33, one launch (start us, length us, event | category | flops | bytes accessed | tf_op | source)
XLA Modules:
  0.0 146.9 jit_solution(10498528209521421996)
XLA Ops:
  0.0 0.0 copy-start
  0.0 0.7 copy-done
  0.7 0.6 broadcast_in_dim.8.lg_ref
  1.2 143.8 %layer.1 = bf16[128,2048]{1,0:T(8,128)(2,1)} custom-call(bf16[128,128]{1,0:T(8,128)(2,1)} %q_in.1, bf16[128,128]{1,0:T(8,128)(2,1)} %k_ref.1, bf16[128,128]{1,0:T(8,128)(2,1)} %v_ref.1, bf16[8,128]{1,0:T(8,128)(2,1)} %broadcast_in_dim.8.lg_ref, bf16[128,2048]{1,0:T(8,128)(2,1)} %res_in.1, bf16[128,2048]{1,0:T(8,128)(2,1)} %ow_ref.1, f32[1,2048]{1,0:T(1,128)} %bitcast.4, ...), custom_call_target="tpu_custom_call" | custom-call | tf_op jit(solution)/shard_map/layer/pallas_call | solution.py:795
  145.0 1.9 %copy.14 = bf16[128,2048]{1,0:T(8,128)(2,1)} copy(bf16[128,2048]{1,0:T(8,128)(2,1)} %layer.1) | data formatting | bytes 1048576
Async XLA Ops:
  0.0 0.7 copy-start
